TPU v7x, 32 devices: a whole 2x2x4 slice. The times are simulated.
32 devices in a mesh: ep: 16 (over z, y, core), tp: 2 (over x).
Axes of the slice: x: 2, y: 2, z: 4, core: 2. Of those that a mesh axis runs over, the one named last changes fastest.
Arguments:
- tokens: bfloat16 [2048, 2048], P('ep'), may hold values from -6 to 6
- expert_ids: int32 [2048, 2], P('ep'), may hold values from 0 to 15, as said below
- route_weights: bfloat16 [2048, 2], P('ep'), may hold values from 0.099609375 to 1
- cotangent: bfloat16 [2048, 2048], P('ep'), may hold values from -3 to 3
- w_gate: bfloat16 [16, 2048, 512], P('ep', None, 'tp'), may hold values from -0.125 to 0.125
- w_up: bfloat16 [16, 2048, 512], P('ep', None, 'tp'), may hold values from -0.125 to 0.125
- w_down: bfloat16 [16, 512, 2048], P('ep', 'tp'), may hold values from -0.25 to 0.25
Outputs:
- token_grad: bfloat16 [2048, 2048], P('ep', 'tp')
- route_grad: bfloat16 [2048, 2], P('ep')
- grad_gate: bfloat16 [16, 2048, 512], P('ep', None, 'tp')
- grad_up: bfloat16 [16, 2048, 512], P('ep', None, 'tp')
- grad_down: bfloat16 [16, 512, 2048], P('ep', 'tp')
- gate_rows: float32 [16, 2048], P('ep')
- up_rows: float32 [16, 2048], P('ep')
- down_rows: float32 [16, 512], P('ep', 'tp')
Inputs may be any that keep to these rules, and one draw needn't show every extreme that they name: `expert_ids`: each row names 2 different experts of one group: both lie in g * 4 to (g + 1) * 4 - 1 for the row's group g. In the rows of one device (aligned blocks of 128 rows) no expert is named more than 32 times, and in every block some expert is named exactly 32 times.
All inputs are finite; a program needn't handle non-finite values.
Results may differ from a plain program's by a relative error of at most 0.012.
Values may be sent and summed in bfloat16 or wider, within the bound.
A program may use at most 64 MiB of HBM per device.

v0:
```python
import functools

import jax
import jax.numpy as jnp
from jax import lax
from jax.experimental import pallas as pl
from jax.experimental.layout import Layout, with_layout_constraint
from jax.experimental.pallas import tpu as pltpu
from jax.sharding import PartitionSpec as P

MESH = pl.DeviceIdType.MESH
LANES = 128
SHARE = 4
GROUPS = 4


def greet(experts, splits, me, col):
    barrier = pltpu.get_barrier_semaphore()

    @pl.loop(1, experts)
    def _(off):
        pl.semaphore_signal(
            barrier, inc=1, device_id={"ep": lax.rem(me + off, experts), "tp": col}, device_id_type=MESH
        )

    for shift in range(1, splits):
        pl.semaphore_signal(
            barrier, inc=1, device_id={"ep": me, "tp": lax.rem(col + shift, splits)}, device_id_type=MESH
        )
    pl.semaphore_wait(barrier, experts - 1 + splits - 1)


def remote(src, dst, send, recv, ep, tp):
    return pltpu.make_async_remote_copy(
        src_ref=src,
        dst_ref=dst,
        send_sem=send,
        recv_sem=recv,
        device_id={"ep": ep, "tp": tp},
        device_id_type=MESH,
    )


def dispatch_kernel(
    experts, splits, rows_ref, cot_ref, choice_ref, scale_ref, rows_out, cot_out, scale_out, landed_choice,
    landed, stage, far_send, far_recv, send, recv, relay_send, relay_recv,
    scale_send, scale_recv, local,
):
    me = lax.axis_index("ep")
    col = lax.axis_index("tp")
    members = experts // GROUPS
    group = me // members
    seat = lax.rem(me, members)
    model_width = rows_out.shape[2]
    capacity = rows_out.shape[1]
    packed = rows_ref.shape[2]
    width = (model_width - packed) // (splits - 1) if splits > 1 else model_width
    shared = model_width - splits * width
    mine = pl.ds(pl.multiple_of(col * width, LANES), width)
    greet(experts, splits, me, col)
    inputs = (rows_ref, cot_ref, choice_ref)
    outputs = (rows_out, cot_out)
    views = [(i, pl.ds(0, width), mine) for i in range(2)]
    if shared:
        views += [(i, pl.ds(width, shared), pl.ds(splits * width, shared)) for i in range(2)]

    def far_copy(step, i):
        there = lax.rem(group + step, GROUPS)
        target = landed_choice.at[step] if i == 2 else landed.at[i, step]
        return remote(
            inputs[i].at[there], target, far_send.at[i, step], far_recv.at[i, step],
            there * members + seat, col,
        )

    def origin(step, hop):
        return lax.rem(group + GROUPS - step, GROUPS) * members + lax.rem(seat + members - hop, members)

    def near_copy(step, hop, n):
        i, here, there = views[n]
        target = lax.rem(seat + hop, members)
        return remote(
            stage.at[i, step, target, :, here], outputs[i].at[origin(step, 0), :, there],
            send.at[n, step, hop], recv.at[n, step, hop], group * members + target, col,
        )

    def own_copy(step, n):
        i, here, there = views[n]
        return pltpu.make_async_copy(
            stage.at[i, step, seat, :, here], outputs[i].at[origin(step, 0), :, there], local.at[n, step]
        )

    def relay(step, hop, shift, i, part):
        block = outputs[i].at[origin(step, hop), :, part]
        peer = lax.rem(col + shift, splits)
        return remote(
            block, block, relay_send.at[i, shift - 1, step, hop], relay_recv.at[i, shift - 1, step, hop], me, peer
        )

    def scale_copy(off):
        there = lax.rem(me + off, experts)
        return remote(
            scale_ref.at[there], scale_out.at[me], scale_send.at[off], scale_recv.at[off], there, col
        )

    scale_own = pltpu.make_async_copy(scale_ref.at[me], scale_out.at[me], local.at[4, 0])
    for step in range(1, GROUPS):
        for i in (2, 0, 1):
            far_copy(step, i).start()
    scale_own.start()
    choice_own = pltpu.make_async_copy(choice_ref.at[group], landed_choice.at[0], local.at[4, 1])
    choice_own.start()

    for step in range(GROUPS):
        if step:
            far_copy(step, 2).wait_recv()
            choice = landed_choice[step]
        else:
            choice = choice_ref[group]
        for i in range(2):
            if step:
                far_copy(step, i).wait_recv()
                block = landed[i, step]
            else:
                block = inputs[i][group]
            spread = lax.dot_general(
                choice, block, (((0,), (0,)), ((), ())), preferred_element_type=jnp.float32
            )
            stage[i, step] = spread.astype(jnp.bfloat16).reshape(members, capacity, packed)
            for n in range(i, len(views), 2):
                own_copy(step, n).start()

            @pl.loop(1, members)
            def _(hop):
                near_copy(step, hop, i).start()

            if shared:

                @pl.loop(1, members)
                def _(hop):
                    near_copy(step, hop, i + 2).start()

        if step == 0:

            @pl.loop(1, experts)
            def _(off):
                scale_copy(off).start()

        for n in range(len(views)):
            own_copy(step, n).wait()
        for i in range(2):
            for shift in range(1, splits):
                relay(step, 0, shift, i, mine).start()

        @pl.loop(1, members)
        def _(hop):
            for i in range(2):
                near_copy(step, hop, i).wait_recv()
                for shift in range(1, splits):
                    relay(step, hop, shift, i, mine).start()

    scale_own.wait()
    choice_own.wait()

    @pl.loop(1, experts)
    def _(off):
        scale_copy(off).wait()

    for step in range(GROUPS):
        if step:
            for i in range(3):
                far_copy(step, i).wait_send()

        @pl.loop(1, members)
        def _(hop):
            for n in range(len(views)):
                near_copy(step, hop, n).wait_send()
                if n >= 2:
                    near_copy(step, hop, n).wait_recv()

        @pl.loop(0, members)
        def _(hop):
            for shift in range(1, splits):
                for i in range(2):
                    relay(step, hop, shift, i, mine).wait_send()
                    peer = lax.rem(col + splits - shift, splits)
                    part = pl.ds(pl.multiple_of(peer * width, LANES), width)
                    relay(step, hop, shift, i, part).wait_recv()


def dispatch(rows, cot, choice, scale, model_width, experts, splits):
    members = experts // GROUPS
    capacity = choice.shape[2] // members
    whole = jax.ShapeDtypeStruct((experts, capacity, model_width), jnp.bfloat16)
    vmem = pl.BlockSpec(memory_space=pltpu.VMEM)
    dma = pltpu.SemaphoreType.DMA
    return pl.pallas_call(
        functools.partial(dispatch_kernel, experts, splits),
        out_shape=(whole, whole, jax.ShapeDtypeStruct(scale.shape, scale.dtype),
                   jax.ShapeDtypeStruct(choice.shape, choice.dtype)),
        in_specs=[vmem] * 4,
        out_specs=(vmem,) * 4,
        scratch_shapes=[
            pltpu.VMEM((2,) + rows.shape, jnp.bfloat16),
            pltpu.VMEM((2, GROUPS, members, capacity, rows.shape[2]), jnp.bfloat16),
            dma((3, GROUPS)),
            dma((3, GROUPS)),
            dma((4, GROUPS, members)),
            dma((4, GROUPS, members)),
            dma((2, splits - 1, GROUPS, members)),
            dma((2, splits - 1, GROUPS, members)),
            dma((experts,)),
            dma((experts,)),
            dma((5, GROUPS)),
        ],
        compiler_params=pltpu.CompilerParams(collective_id=0, has_side_effects=True),
    )(rows, cot, choice, scale)


def combine_kernel(
    experts, splits, part_ref, route_ref, square_ref, choice_ref, back, back_route, square_out,
    peer_part, total, gathered, finished, peer_route, route_total,
    swap_send, swap_recv, small_send, small_recv, near_send, near_recv, far_send, far_recv,
    route_send, route_recv,
):
    me = lax.axis_index("ep")
    col = lax.axis_index("tp")
    members = experts // GROUPS
    group = me // members
    seat = lax.rem(me, members)
    capacity = part_ref.shape[1]
    width = back.shape[2]
    mine = pl.ds(pl.multiple_of(col * width, LANES), width)
    greet(experts, splits, me, col)
    order = tuple(range(1, GROUPS)) + (0,)

    def home(step, hop):
        return lax.rem(group + GROUPS - step, GROUPS) * members + lax.rem(seat + hop, members)

    def swap(step, hop, shift):
        source = home(step, hop)
        peer = lax.rem(col + shift, splits)
        theirs = pl.ds(pl.multiple_of(peer * width, LANES), width)
        return remote(
            part_ref.at[source, :, theirs], peer_part.at[shift - 1, source],
            swap_send.at[shift - 1, step, hop], swap_recv.at[shift - 1, step, hop], me, peer,
        )

    small = []
    for shift in range(1, splits):
        peer = lax.rem(col + shift, splits)
        small.append((
            remote(route_ref, peer_route.at[shift - 1], small_send.at[0, shift - 1],
                   small_recv.at[0, shift - 1], me, peer),
            remote(square_ref, square_out.at[shift - 1], small_send.at[1, shift - 1],
                   small_recv.at[1, shift - 1], me, peer),
        ))
    for shift in range(1, splits):
        small[shift - 1][0].start()

    for step in order:

        @pl.loop(1, members + 1)
        def _(turn):
            for shift in range(1, splits):
                swap(step, lax.rem(turn, members), shift).start()

    for shift in range(1, splits):
        small[shift - 1][1].start()

    def block_total(step, hop):
        source = home(step, hop)
        for shift in range(1, splits):
            swap(step, hop, shift).wait_recv()
        value = part_ref[source, :, mine].astype(jnp.float32)
        for shift in range(1, splits):
            value = value + peer_part[shift - 1, source].astype(jnp.float32)
        return value.astype(back.dtype)

    def near_copy(step, hop):
        target = lax.rem(seat + hop, members)
        return remote(
            total.at[step, hop], gathered.at[step, seat],
            near_send.at[step, hop], near_recv.at[step, hop], group * members + target, col,
        )

    def far_copy(step):
        return remote(
            finished.at[step], back.at[group], far_send.at[step], far_recv.at[step], home(step, 0), col
        )

    def route_copy(off):
        there = lax.rem(me + off, experts)
        return remote(
            route_total.at[there], back_route.at[me], route_send.at[off], route_recv.at[off], there, col
        )

    value = route_ref[...]
    for shift in range(1, splits):
        small[shift - 1][0].wait_recv()
        value = value + peer_route[shift - 1]
    route_total[...] = value
    back_route[me] = route_total[me]

    @pl.loop(1, experts)
    def _(off):
        route_copy(off).start()

    def spread(step):
        @pl.loop(1, members)
        def _(hop):
            total[step, hop] = block_total(step, hop)
            near_copy(step, hop).start()

        gathered[step, seat] = block_total(step, 0)

    def collect(step):
        @pl.loop(1, members)
        def _(hop):
            near_copy(step, hop).wait_recv()

        pairs = gathered[step].reshape(members * capacity, width)
        summed = jnp.dot(choice_ref[step], pairs, preferred_element_type=jnp.float32).astype(back.dtype)
        if step:
            finished[step] = summed
            far_copy(step).start()
        else:
            back[group] = summed

    for turn, step in enumerate(order):
        spread(step)
        if turn:
            collect(order[turn - 1])
    collect(order[-1])

    @pl.loop(1, experts)
    def _(off):
        route_copy(off).wait()

    for step in range(GROUPS):
        if step:
            far_copy(step).wait()

        @pl.loop(1, members)
        def _(hop):
            near_copy(step, hop).wait_send()

        @pl.loop(0, members)
        def _(hop):
            for shift in range(1, splits):
                swap(step, hop, shift).wait_send()

    for shift in range(1, splits):
        small[shift - 1][0].wait_send()
        small[shift - 1][1].wait()


def combine(part, route, squares, choice, experts, splits):
    capacity, model_width = part.shape[1:]
    width = model_width // splits
    members = experts // GROUPS
    group_cap = choice.shape[1]
    vmem = pl.BlockSpec(memory_space=pltpu.VMEM)
    dma = pltpu.SemaphoreType.DMA
    return pl.pallas_call(
        functools.partial(combine_kernel, experts, splits),
        out_shape=(
            jax.ShapeDtypeStruct((GROUPS, group_cap, width), jnp.bfloat16),
            jax.ShapeDtypeStruct(route.shape, jnp.float32),
            jax.ShapeDtypeStruct((splits - 1,) + squares.shape, jnp.float32),
        ),
        in_specs=[vmem] * 4,
        out_specs=(vmem,) * 3,
        scratch_shapes=[
            pltpu.VMEM((splits - 1, experts, capacity, width), jnp.bfloat16),
            pltpu.VMEM((GROUPS, members, capacity, width), jnp.bfloat16),
            pltpu.VMEM((GROUPS, members, capacity, width), jnp.bfloat16),
            pltpu.VMEM((GROUPS, group_cap, width), jnp.bfloat16),
            pltpu.VMEM((splits - 1,) + route.shape, jnp.float32),
            pltpu.VMEM(route.shape, jnp.float32),
            dma((splits - 1, GROUPS, members)),
            dma((splits - 1, GROUPS, members)),
            dma((2, splits - 1)),
            dma((2, splits - 1)),
            dma((GROUPS, members)),
            dma((GROUPS, members)),
            dma((GROUPS,)),
            dma((GROUPS,)),
            dma((experts,)),
            dma((experts,)),
        ],
        compiler_params=pltpu.CompilerParams(collective_id=1, has_side_effects=True),
    )(part, route, squares, choice)


def on_device(tokens, expert_ids, route_weights, cotangent, w_gate, w_up, w_down):
    tok_rows, model_width = tokens.shape
    topk = expert_ids.shape[1]
    experts = lax.axis_size("ep")
    splits = lax.axis_size("tp")
    capacity = 2 * tok_rows * topk // experts
    slot_count = experts * capacity
    f32, bf16 = jnp.float32, jnp.bfloat16

    expert_iota = jnp.arange(experts, dtype=jnp.int32)[None, :]
    slots = jnp.arange(slot_count, dtype=jnp.int32)[None, :]
    slot_expert = slots // capacity
    spread = (expert_iota.reshape(experts, 1) == slot_expert).astype(bf16)
    picks = [expert_ids[:, k : k + 1] == expert_iota for k in range(topk)]
    member = sum(p.astype(f32) for p in picks)
    weight = sum(
        jnp.where(p, route_weights[:, k : k + 1].astype(f32), 0.0) for k, p in enumerate(picks)
    ).astype(bf16)
    order = jnp.arange(tok_rows, dtype=jnp.int32)
    earlier = (order[:, None] > order[None, :]).astype(bf16)
    before = jnp.dot(earlier, member.astype(bf16), preferred_element_type=f32)
    rank = jnp.where(member > 0, before, -1.0).astype(bf16)
    slot_rank = jnp.dot(rank, spread, preferred_element_type=f32)
    chosen = slot_rank == (slots % capacity).astype(f32)
    select = chosen.astype(bf16)
    slot_weight = jnp.sum(
        jnp.where(chosen, jnp.dot(weight, spread, preferred_element_type=f32), 0.0), axis=0
    )
    members = experts // GROUPS
    group_cap = members * capacity // topk
    group_slots = jnp.arange(GROUPS * group_cap, dtype=jnp.int32)[None, :]
    group_iota = jnp.arange(GROUPS, dtype=jnp.int32)[None, :]
    in_group = expert_ids[:, :1] // members == group_iota
    group_before = jnp.dot(earlier, in_group.astype(bf16), preferred_element_type=f32)
    own_rank = jnp.sum(jnp.where(in_group, group_before, 0.0), axis=1, keepdims=True).astype(jnp.int32)
    own_slot = expert_ids[:, :1] // members * group_cap + own_rank
    group_select = (own_slot == group_slots).astype(bf16)
    grouped = lax.dot_general(
        group_select, select, (((0,), (0,)), ((), ())), preferred_element_type=f32
    ).astype(bf16)
    span = members * capacity
    choice = jnp.stack(
        [
            grouped[g * group_cap : (g + 1) * group_cap, g * span : (g + 1) * span]
            for g in range(GROUPS)
        ]
    )
    width = model_width // splits
    shared = model_width // SHARE // (splits * LANES) * (splits * LANES) if SHARE else 0
    cut = (model_width - shared) // splits
    start = lax.axis_index("tp") * cut

    def pack(array):
        piece = jnp.concatenate(
            [lax.dynamic_slice_in_dim(array, start, cut, 1), array[:, splits * cut :]], axis=1
        )
        packed = lax.dot_general(
            group_select, piece, (((0,), (0,)), ((), ())), preferred_element_type=f32
        )
        return packed.astype(bf16).reshape(GROUPS, group_cap, cut + shared)

    lane_pad = -capacity % LANES
    scale_out = jnp.pad(slot_weight.reshape(experts, 1, capacity), ((0, 0), (0, 0), (0, lane_pad)))
    slot_rows, slot_cot, got_scale, got_choice = dispatch(
        pack(tokens), pack(cotangent), choice, scale_out, model_width, experts, splits
    )
    slot_rows = slot_rows.reshape(slot_count, model_width)
    slot_cot = slot_cot.reshape(slot_count, model_width)
    scale_col = got_scale[:, 0, :capacity].reshape(slot_count, 1)

    gate_cols = w_gate[0]
    up_cols = w_up[0]
    down_part = w_down[0]
    gate_pre = jnp.dot(slot_rows, gate_cols, preferred_element_type=f32)
    up_pre = jnp.dot(slot_rows, up_cols, preferred_element_type=f32)
    hidden_back = lax.dot_general(
        slot_cot, down_part, (((1,), (1,)), ((), ())), preferred_element_type=f32
    )
    gate_sig = jax.nn.sigmoid(gate_pre)
    activated = gate_pre * gate_sig
    hidden = activated * up_pre
    route_part = jnp.sum(hidden * hidden_back, axis=1)
    hidden_cot = scale_col * hidden_back
    up_cot = (hidden_cot * activated).astype(bf16)
    gate_cot = (hidden_cot * up_pre * gate_sig * (1.0 + gate_pre * (1.0 - gate_sig))).astype(bf16)
    weighted_hidden = (scale_col * hidden).astype(bf16)

    def outer(left, right):
        return lax.dot_general(
            left, right, (((0,), (0,)), ((), ())), preferred_element_type=f32
        ).astype(bf16)

    grad_down = outer(weighted_hidden, slot_cot)
    by_rows = Layout(major_to_minor=(0, 1))
    grad_gate = with_layout_constraint(outer(slot_rows, gate_cot), by_rows)
    grad_up = with_layout_constraint(outer(slot_rows, up_cot), by_rows)
    token_term = lax.dot_general(
        gate_cot, gate_cols, (((1,), (1,)), ((), ())), preferred_element_type=f32
    )
    token_term = token_term + lax.dot_general(
        up_cot, up_cols, (((1,), (1,)), ((), ())), preferred_element_type=f32
    )
    gate_square = jnp.sum(jnp.square(grad_gate.astype(f32)), axis=1)
    up_square = jnp.sum(jnp.square(grad_up.astype(f32)), axis=1)
    down_square = jnp.sum(jnp.square(grad_down.astype(f32)), axis=1)
    squares = jnp.stack([gate_square, up_square])
    route_out = jnp.pad(route_part.reshape(experts, 1, capacity), ((0, 0), (0, 0), (0, lane_pad)))
    back_rows, back_route, peer_squares = combine(
        token_term.astype(bf16).reshape(experts, capacity, model_width),
        route_out, squares, got_choice, experts, splits,
    )
    squares = squares + jnp.sum(peer_squares, axis=0)
    token_grad = jnp.dot(
        group_select, back_rows.reshape(GROUPS * group_cap, width), preferred_element_type=f32
    ).astype(bf16)
    slot_route = back_route[:, 0, :capacity].reshape(1, slot_count)
    route_grad = jnp.concatenate(
        [
            jnp.sum(
                jnp.where(chosen & (slot_expert == expert_ids[:, k : k + 1]), slot_route, 0.0),
                axis=1, keepdims=True,
            )
            for k in range(topk)
        ],
        axis=1,
    ).astype(bf16)
    return (
        token_grad,
        route_grad,
        grad_gate[None],
        grad_up[None],
        grad_down[None],
        squares[0:1],
        squares[1:2],
        down_square[None],
    )


def solution(mesh):
    return jax.shard_map(
        on_device,
        mesh=mesh,
        in_specs=(
            P("ep", None),
            P("ep", None),
            P("ep", None),
            P("ep", None),
            P("ep", None, "tp"),
            P("ep", None, "tp"),
            P("ep", "tp", None),
        ),
        out_specs=(
            P("ep", "tp"),
            P("ep", None),
            P("ep", None, "tp"),
            P("ep", None, "tp"),
            P("ep", "tp", None),
            P("ep", None),
            P("ep", None),
            P("ep", "tp"),
        ),
        check_vma=False,
    )
```

profile of v0, /device:TPU:0, one launch (start us, length us, event | category | flops | bytes accessed | tf_op | source)
XLA Modules:
  0.0 126.4 jit_solution(13056355829028642269)
XLA Ops:
  0.7 0.8 bitcast_convert_fusion.1
  1.5 0.8 slice_bitcast_fusion.5
  2.3 0.1 fusion.2
  2.5 0.4 convolution_compare_fusion
  2.9 0.3 fusion
  3.1 0.1 reshape.108
  3.2 0.6 pad.7.scale_ref
  3.8 0.3 convolution_convert_fusion.5
  4.2 0.6 pad_maximum_fusion.choice_ref
  4.9 1.3 %convolution_convert_fusion.3 = bf16[256,1280]{1,0:T(8,128)(2,1)} fusion(bf16[128,512]{1,0:T(8,128)(2,1)S(1)} %slice-done.1, bf16[128,768]{1,0:T(8,128)(2,1)S(1)} %get-tuple-element.44, s32[128]{0:T(128)S(1)} %fusion.52), kind=kOutput, calls=%fused_computation.4 | convolution fusion | flops 84901888 | bytes 983552 | tf_op jit(solution)/shard_map/dot_general | solution.py:451
  6.2 1.3 %convolution_convert_fusion.4 = bf16[256,1280]{1,0:T(8,128)(2,1)} fusion(bf16[128,512]{1,0:T(8,128)(2,1)S(1)} %slice-done, bf16[128,768]{1,0:T(8,128)(2,1)S(1)} %get-tuple-element.45, s32[128]{0:T(128)S(1)} %fusion.52), kind=kOutput, calls=%fused_computation.5 | convolution fusion | flops 84901888 | bytes 983552 | tf_op jit(solution)/shard_map/dot_general | solution.py:451
  7.5 55.0 %shard_map.134 = (bf16[16,32,2048]{2,1,0:T(8,128)(2,1)}, bf16[16,32,2048]{2,1,0:T(8,128)(2,1)}, f32[16,1,128]{2,1,0:T(1,128)}, bf16[4,64,128]{2,1,0:T(8,128)(2,1)}) custom-call(bf16[4,64,1280]{2,1,0:T(8,128)(2,1)} %bitcast.74, bf16[4,64,1280]{2,1,0:T(8,128)(2,1)} %bitcast.73, bf16[4,64,128]{2,1,0:T(8,128)(2,1)} %pad_maximum_fusion.choice_ref, ...), custom_call_target="tpu_custom_call" | custom-call | tf_op jit(solution)/shard_map/pallas_call | solution.py:196
  62.5 0.8 slice_reduce_fusion.1
  63.4 2.5 %fusion.5 = f32[512,256]{0,1:T(8,128)S(1)} fusion(bf16[512,2048]{1,0:T(8,128)(2,1)} %bitcast.83, bf16[1,2048,256]{2,1,0:T(8,128)(2,1)S(1)} %copy-done), kind=kOutput, calls=%fused_computation.20 | convolution fusion | flops 536870912 | bytes 3670016 | tf_op jit(solution)/shard_map/dot_general | solution.py:468
  65.9 0.8 fusion.8
  66.7 0.8 copy-done.6
  67.5 0.3 copy-done.7
  67.8 1.0 multiply_reduce_fusion.3
  68.7 2.3 %multiply_reduce_fusion = (f32[256]{0:T(256)}, bf16[256,2048]{1,0:T(8,128)(2,1)}) fusion(bf16[512,2048]{1,0:T(8,128)(2,1)S(1)} %bitcast.88, f32[512]{0:T(512)S(1)} %mul.52, f32[512,256]{0,1:T(8,128)S(1)} %fusion.8, f32[512,256]{0,1:T(8,128)S(1)} %fusion.5), kind=kOutput, calls=%fused_computation.6 | convolution fusion | flops 539885312 | bytes 4197376 | tf_op jit(solution)/shard_map/dot_general | solution.py:483
  71.1 0.6 pad.8.route_ref
  71.7 3.6 %multiply_reduce_fusion.2 = (f32[2048]{0:T(1024)S(1)}, bf16[2048,256]{1,0:T(8,128)(2,1)}) fusion(bf16[512,2048]{1,0:T(8,128)(2,1)} %bitcast.84, bf16[512,256]{0,1:T(8,128)(2,1)S(1)} %get-tuple-element.25), kind=kOutput, calls=%fused_computation.8 | convolution fusion | flops 538966016 | bytes 3416064 | tf_op jit(solution)/shard_map/dot_general | solution.py:483
  75.3 1.8 %multiply_reduce_fusion.1 = (f32[2048]{0:T(1024)S(1)}, bf16[2048,256]{1,0:T(8,128)(2,1)}) fusion(bf16[512,2048]{1,0:T(8,128)(2,1)S(1)} %bitcast.86, bf16[512,256]{0,1:T(8,128)(2,1)S(1)} %get-tuple-element.26), kind=kOutput, calls=%fused_computation.7 | convolution fusion | flops 538966016 | bytes 3416064 | tf_op jit(solution)/shard_map/dot_general | solution.py:483
  77.1 0.6 pad_maximum_fusion.1.square_ref
  77.7 0.8 fusion.3
  78.5 2.2 %add_convert_fusion = bf16[512,2048]{1,0:T(8,128)(2,1)} fusion(f32[512,2048]{1,0:T(8,128)S(1)} %fusion.3, bf16[512,256]{0,1:T(8,128)(2,1)S(1)} %get-tuple-element.26, bf16[1,2048,256]{2,1,0:T(8,128)(2,1)S(1)} %copy-done.1), kind=kOutput, calls=%fused_computation | convolution fusion | flops 538968064 | bytes 7602176 | tf_op jit(solution)/shard_map/dot_general | solution.py:494
  80.7 40.7 %shard_map.135 = (bf16[4,64,1024]{2,1,0:T(8,128)(2,1)}, f32[16,1,128]{2,1,0:T(1,128)}, f32[1,2,2048]{2,1,0:T(2,128)}) custom-call(bf16[16,32,2048]{2,1,0:T(8,128)(2,1)} %bitcast.72, f32[16,1,128]{2,1,0:T(1,128)} %pad.8.route_ref, f32[2,2048]{1,0:T(2,128)} %pad_maximum_fusion.1.square_ref, bf16[4,64,128]{2,1,0:T(8,128)(2,1)} %get-tuple-element.18.choice_ref), custom_call_target="tpu_custom_call" | custom-call | tf_op jit(solution)/shard_map/pallas_call | solution.py:364
  121.4 0.7 bitcast_add_fusion
  122.1 2.0 %convolution_convert_fusion.6 = bf16[128,1024]{1,0:T(8,128)(2,1)} fusion(bf16[256,1024]{1,0:T(8,128)(2,1)} %bitcast.75, s32[128]{0:T(128)S(1)} %fusion.52), kind=kOutput, calls=%fused_computation.10 | convolution fusion | flops 67272704 | bytes 786944 | tf_op jit(solution)/shard_map/dot_general | solution.py:507
  124.2 0.6 fusion.59
  124.8 0.7 slice_reduce_fusion
  125.6 0.3 select_reduce_fusion.1
  125.8 0.5 pad_maximum_fusion.2
  (25 shorter events, 0.4 us)
Async XLA Ops:
  0.6 62.7 %copy-start = (bf16[1,2048,256]{2,1,0:T(8,128)(2,1)S(1)}, bf16[1,2048,256]{2,1,0:T(8,128)(2,1)}, u32[]{:S(2)}) copy-start(bf16[1,2048,256]{2,1,0:T(8,128)(2,1)} %param.11) | copy-start | bytes 3145732
  0.6 4.2 %copy-start.3 = (bf16[128,2048]{1,0:T(8,128)(2,1)S(1)}, bf16[128,2048]{1,0:T(8,128)(2,1)}, u32[]{:S(2)}) copy-start(bf16[128,2048]{1,0:T(8,128)(2,1)} %param.10) | copy-start | bytes 1572868
  0.7 4.2 %slice-start.1 = ((bf16[128,2048]{1,0:T(8,128)(2,1)}), bf16[128,512]{1,0:T(8,128)(2,1)S(1)}, s32[]{:S(2)}) async-start(bf16[128,2048]{1,0:T(8,128)(2,1)} %param.10), calls=%async_computation.1 | async-start | bytes 262144 | tf_op jit(solution)/shard_map/slice | solution.py:449
  0.7 4.2 %copy-start.2 = (bf16[128,2048]{1,0:T(8,128)(2,1)S(1)}, bf16[128,2048]{1,0:T(8,128)(2,1)}, u32[]{:S(2)}) copy-start(bf16[128,2048]{1,0:T(8,128)(2,1)} %param.7) | copy-start | bytes 1572868
  0.7 5.5 %slice-start = ((bf16[128,2048]{1,0:T(8,128)(2,1)}), bf16[128,512]{1,0:T(8,128)(2,1)S(1)}, s32[]{:S(2)}) async-start(bf16[128,2048]{1,0:T(8,128)(2,1)} %param.7), calls=%async_computation | async-start | bytes 262144 | tf_op jit(solution)/shard_map/slice | solution.py:449
  62.5 3.4 %copy-start.1 = (bf16[1,2048,256]{2,1,0:T(8,128)(2,1)S(1)}, bf16[1,2048,256]{2,1,0:T(8,128)(2,1)}, u32[]{:S(2)}) copy-start(bf16[1,2048,256]{2,1,0:T(8,128)(2,1)} %param.12) | copy-start | bytes 3145732
  63.4 2.5 %copy-start.4 = (bf16[16,32,2048]{2,1,0:T(8,128)(2,1)S(1)}, bf16[16,32,2048]{2,1,0:T(8,128)(2,1)}, u32[]{:S(2)}) copy-start(bf16[16,32,2048]{2,1,0:T(8,128)(2,1)} %get-tuple-element.17) | copy-start | bytes 6291460
  65.9 1.6 %copy-start.6 = (bf16[16,32,2048]{2,1,0:T(8,128)(2,1)S(1)}, bf16[16,32,2048]{2,1,0:T(8,128)(2,1)}, u32[]{:S(2)}) copy-start(bf16[16,32,2048]{2,1,0:T(8,128)(2,1)} %get-tuple-element.16) | copy-start | bytes 6291460
  65.9 1.8 %copy-start.7 = (bf16[1,256,2048]{2,1,0:T(8,128)(2,1)S(1)}, bf16[1,256,2048]{2,1,0:T(8,128)(2,1)}, u32[]{:S(2)}) copy-start(bf16[1,256,2048]{2,1,0:T(8,128)(2,1)} %param.13) | copy-start | bytes 3145732
  71.7 3.6 %copy-start.5 = (bf16[16,32,2048]{2,1,0:T(8,128)(2,1)S(1)}, bf16[16,32,2048]{2,1,0:T(8,128)(2,1)}, u32[]{:S(2)}) copy-start(bf16[16,32,2048]{2,1,0:T(8,128)(2,1)} %get-tuple-element.17) | copy-start | bytes 6291460
where the time goes:
time: 127 us; the launch traced here: 126 us
  Pallas kernels  95.7 us (75%)
  matrix products  20.6 us (16%)
  local copies, waits for them, and re-layouts  4.85 us (4%)
  other arithmetic  4.39 us (3%)
    pallas_call x1, Pallas kernels, dispatch(): pl.pallas_call(functools.partial(dispatch_kernel, experts, splits), out_s...  55 us
    pallas_call x1, Pallas kernels, combine(): pl.pallas_call(functools.partial(combine_kernel, experts, splits), out_sh...  40.7 us
    dot_general x3, matrix products, outer(): lax.dot_general(left, right, (((0,), (0,)), ((), ())), preferred_element_...  7.7 us
    dot_general x2, matrix products, pack(): lax.dot_general(group_select, piece, (((0,), (0,)), ((), ())), preferred_...  2.57 us

commit v1 on v0

v1 whole, which is shorter than its diff:
```python
import functools

import jax
import jax.numpy as jnp
from jax import lax
from jax.experimental import pallas as pl
from jax.experimental.layout import Layout, with_layout_constraint
from jax.experimental.pallas import tpu as pltpu
from jax.sharding import PartitionSpec as P

MESH = pl.DeviceIdType.MESH
LANES = 128
TILE = 256
SHARED = (0, 4, 2, 2)
GROUPS = 4


def greet(experts, splits, me, col):
    barrier = pltpu.get_barrier_semaphore()

    @pl.loop(1, experts)
    def _(off):
        pl.semaphore_signal(
            barrier, inc=1, device_id={"ep": lax.rem(me + off, experts), "tp": col}, device_id_type=MESH
        )

    for shift in range(1, splits):
        pl.semaphore_signal(
            barrier, inc=1, device_id={"ep": me, "tp": lax.rem(col + shift, splits)}, device_id_type=MESH
        )
    return barrier


def remote(src, dst, send, recv, ep, tp):
    return pltpu.make_async_remote_copy(
        src_ref=src,
        dst_ref=dst,
        send_sem=send,
        recv_sem=recv,
        device_id={"ep": ep, "tp": tp},
        device_id_type=MESH,
    )


def partner(group, step):
    if step == 0:
        return group
    if step == 1:
        return group + 1 - 2 * lax.rem(group, 2)
    if step == 2:
        return lax.rem(group + 2, GROUPS)
    return GROUPS - 1 - group


def column_plan(model_width, splits):
    plan = []
    for eighths in SHARED:
        shared = model_width * eighths // 8 // (splits * LANES) * (splits * LANES) if splits == 2 else 0
        cut = (model_width - shared) // splits
        plan.append((cut, cut + shared))
    return plan


def layer_kernel(
    experts, splits,
    tokens_ref, cot_ref, gsel_ref, choice_ref, scale_ref, gate_hbm, up_hbm, down_hbm,
    token_out, back_route, gate_out, up_out, square_out, down_out, down_square_out,
    packed, landed, landed_choice, stage, rows, scale_in, wide, down, cots, weighted,
    part, peer_part, total, gathered, finished, back, route_mine, peer_route, route_total,
    square_mine, peer_square, down_acc,
    far_send, far_recv, near_send, near_recv, relay_send, relay_recv, scale_send, scale_recv,
    swap_send, swap_recv, join_send, join_recv, home_send, home_recv, small_send, small_recv,
    route_send, route_recv, square_send, square_recv, local,
):
    me = lax.axis_index("ep")
    col = lax.axis_index("tp")
    members = experts // GROUPS
    group = me // members
    seat = lax.rem(me, members)
    model_width = tokens_ref.shape[1]
    capacity = rows.shape[3]
    span = members * capacity
    hidden_width = down.shape[0]
    width = model_width // splits
    f32, bf16 = jnp.float32, jnp.bfloat16
    plan = column_plan(model_width, splits)
    places = [partner(group, step) for step in range(GROUPS)]
    barrier = greet(experts, splits, me, col)
    inputs = (tokens_ref, cot_ref)

    weight_loads = (
        pltpu.make_async_copy(gate_hbm, wide.at[:, pl.ds(0, hidden_width)], local.at[0]),
        pltpu.make_async_copy(up_hbm, wide.at[:, pl.ds(hidden_width, hidden_width)], local.at[1]),
        pltpu.make_async_copy(down_hbm, down, local.at[2]),
    )
    for load in weight_loads:
        load.start()

    def window(step):
        cut, wide_cut = plan[step]
        return pl.ds(pl.multiple_of(col * cut, LANES), wide_cut)

    def relay_part(step, which):
        cut, wide_cut = plan[step]
        return pl.ds(pl.multiple_of(which * wide_cut, LANES), cut)

    def around(hop):
        return lax.rem(seat + hop, members)

    def before(hop):
        return lax.rem(seat + members - hop, members)

    def far_copy(step, i):
        if i == 2:
            source, target = choice_ref.at[places[step]], landed_choice.at[step]
        else:
            cols = pl.ds(0, plan[step][1])
            source, target = packed.at[i, step, :, cols], landed.at[i, step, :, cols]
        return remote(
            source, target, far_send.at[i, step], far_recv.at[i, step],
            places[step] * members + seat, col,
        )

    def scale_copy(step, hop):
        there = places[step] * members + around(hop)
        return remote(
            scale_ref.at[there], scale_in.at[step, seat],
            scale_send.at[step, hop], scale_recv.at[step, hop], there, col,
        )

    def near_copy(step, hop, i):
        if step == 0:
            source = stage.at[i, 0, around(hop), :, window(0)]
        else:
            source = stage.at[i, step, around(hop), :, pl.ds(0, plan[step][1])]
        return remote(
            source, rows.at[i, step, seat, :, window(step)],
            near_send.at[i, step, hop], near_recv.at[i, step, hop], group * members + around(hop), col,
        )

    def relay(step, hop, shift, i, which):
        block = rows.at[i, step, before(hop), :, relay_part(step, which)]
        return remote(
            block, block, relay_send.at[i, shift - 1, step, hop], relay_recv.at[i, shift - 1, step, hop],
            me, lax.rem(col + shift, splits),
        )

    def swap(step, hop, shift):
        peer = lax.rem(col + shift, splits)
        theirs = pl.ds(pl.multiple_of(peer * width, LANES), width)
        return remote(
            part.at[step, around(hop), :, theirs], peer_part.at[shift - 1, step, around(hop)],
            swap_send.at[shift - 1, step, hop], swap_recv.at[shift - 1, step, hop], me, peer,
        )

    def small_route(step, shift):
        return remote(
            route_mine.at[step], peer_route.at[shift - 1, step],
            small_send.at[shift - 1, step], small_recv.at[shift - 1, step],
            me, lax.rem(col + shift, splits),
        )

    def small_square(shift):
        return remote(
            square_mine, peer_square.at[shift - 1], square_send.at[shift - 1], square_recv.at[shift - 1],
            me, lax.rem(col + shift, splits),
        )

    def join_copy(step, hop):
        return remote(
            total.at[step, hop], gathered.at[step, seat],
            join_send.at[step, hop], join_recv.at[step, hop], group * members + around(hop), col,
        )

    def home_copy(step):
        return remote(
            finished.at[step], back.at[group], home_send.at[step], home_recv.at[step],
            places[step] * members + seat, col,
        )

    def route_copy(step, hop):
        there = places[step] * members + around(hop)
        return remote(
            route_total.at[step], back_route.at[me], route_send.at[step, hop], route_recv.at[step, hop],
            there, col,
        )

    def pack(step, i):
        source = inputs[i][:, window(step)] if step else inputs[i][...]
        return jnp.dot(gsel_ref[places[step]], source, preferred_element_type=f32).astype(bf16)

    def spread(step, i, block):
        choice = landed_choice[step] if step else choice_ref[group]
        value = lax.dot_general(choice, block, (((0,), (0,)), ((), ())), preferred_element_type=f32)
        wide_cut = block.shape[1]
        stage[i, step, :, :, pl.ds(0, wide_cut)] = value.astype(bf16).reshape(members, capacity, wide_cut)

        @pl.loop(1, members)
        def _(hop):
            near_copy(step, hop, i).start()

        cols = window(step) if step else pl.ds(0, wide_cut)
        rows[i, step, seat, :, cols] = stage[i, step, seat, :, pl.ds(0, wide_cut)]
        if step:
            for shift in range(1, splits):
                relay(step, 0, shift, i, col).start()

    def arrive(step, i):
        if i == 0:
            far_copy(step, 2).wait_recv()
        far_copy(step, i).wait_recv()
        spread(step, i, landed[i, step, :, pl.ds(0, plan[step][1])])

    def forward(step, i):
        @pl.loop(1, members)
        def _(hop):
            near_copy(step, hop, i).wait_recv()
            for shift in range(1, splits):
                relay(step, hop, shift, i, col).start()

    def complete(step):
        @pl.loop(0 if step else 1, members)
        def _(hop):
            for shift in range(1, splits):
                for i in range(2):
                    relay(step, hop, shift, i, lax.rem(col + splits - shift, splits)).wait_recv()

        @pl.loop(0 if step else 1, members)
        def _(hop):
            scale_copy(step, hop).wait_recv()

    def compute(step):
        slot_rows = rows[0, step].reshape(span, model_width)
        slot_cot = rows[1, step].reshape(span, model_width)
        pre = jnp.dot(slot_rows, wide[...], preferred_element_type=f32)
        gate_pre, up_pre = pre[:, :hidden_width], pre[:, hidden_width:]
        hidden_back = lax.dot_general(
            slot_cot, down[...], (((1,), (1,)), ((), ())), preferred_element_type=f32
        )
        spread_scale = jnp.broadcast_to(scale_in[step], (members, capacity, LANES))
        lane = lax.broadcasted_iota(jnp.int32, (members, capacity, LANES), 2)
        slot = lax.broadcasted_iota(jnp.int32, (members, capacity, LANES), 1)
        scale = jnp.sum(jnp.where(lane == slot, spread_scale, 0.0), axis=2, keepdims=True)
        scale = scale.reshape(span, 1)
        gate_sig = jax.nn.sigmoid(gate_pre)
        activated = gate_pre * gate_sig
        hidden = activated * up_pre
        route = hidden * hidden_back
        folded = route[:, :LANES]
        for start in range(LANES, hidden_width, LANES):
            folded = folded + route[:, start : start + LANES]
        route_mine[step] = jnp.sum(folded.T, axis=0, keepdims=True)
        hidden_cot = scale * hidden_back
        up_cot = (hidden_cot * activated).astype(bf16)
        gate_cot = (hidden_cot * up_pre * gate_sig * (1.0 + gate_pre * (1.0 - gate_sig))).astype(bf16)
        slots = pl.ds(step * span, span)
        cots[slots, pl.ds(0, hidden_width)] = gate_cot
        cots[slots, pl.ds(hidden_width, hidden_width)] = up_cot
        weighted[slots, :] = (scale * hidden).astype(bf16)
        both = cots[slots, :]

        @pl.loop(0, model_width // (2 * TILE))
        def _(tile):
            cols = pl.ds(pl.multiple_of(tile * 2 * TILE, LANES), 2 * TILE)
            term = lax.dot_general(
                both, wide[cols, :], (((1,), (1,)), ((), ())), preferred_element_type=f32
            )
            part[step, :, :, cols] = term.astype(bf16).reshape(members, capacity, 2 * TILE)

        for shift in range(1, splits):
            small_route(step, shift).start()

    def send_swaps(step):
        @pl.loop(1, members + 1)
        def _(turn):
            for shift in range(1, splits):
                swap(step, lax.rem(turn, members), shift).start()

    def route_home(step):
        value = route_mine[step]
        for shift in range(1, splits):
            small_route(step, shift).wait_recv()
            value = value + peer_route[shift - 1, step]
        route_total[step] = value
        if step == 0:
            back_route[me] = value

        @pl.loop(0 if step else 1, members)
        def _(hop):
            route_copy(step, hop).start()

    def block_total(step, hop):
        source = around(hop)
        for shift in range(1, splits):
            swap(step, hop, shift).wait_recv()
        mine = pl.ds(pl.multiple_of(col * width, LANES), width)
        value = part[step, source, :, mine].astype(f32)
        for shift in range(1, splits):
            value = value + peer_part[shift - 1, step, source].astype(f32)
        return value.astype(bf16)

    def reduce(step):
        @pl.loop(1, members)
        def _(hop):
            total[step, hop] = block_total(step, hop)
            join_copy(step, hop).start()

        gathered[step, seat] = block_total(step, 0)

    def collect(step):
        @pl.loop(1, members)
        def _(hop):
            join_copy(step, hop).wait_recv()

        pairs = gathered[step].reshape(span, width)
        choice = landed_choice[step] if step else choice_ref[group]
        summed = jnp.dot(choice, pairs, preferred_element_type=f32).astype(bf16)
        if step:
            finished[step] = summed
            home_copy(step).start()
        else:
            back[group] = summed

    def lane_sums(value):
        folded = value[:, :LANES]
        for start in range(LANES, value.shape[1], LANES):
            folded = folded + value[:, start : start + LANES]
        return folded

    def grads_in():
        @pl.loop(0, model_width // TILE)
        def _(tile):
            cols = pl.ds(pl.multiple_of(tile * TILE, LANES), TILE)
            left = rows[0, :, :, :, cols].reshape(GROUPS * span, TILE)
            grad = lax.dot_general(
                left, cots[...], (((0,), (0,)), ((), ())), preferred_element_type=f32
            ).astype(bf16)
            for n, out in enumerate((gate_out, up_out)):
                value = grad[:, n * hidden_width : (n + 1) * hidden_width]
                out[cols, :] = value
                square = lane_sums(jnp.square(value.astype(f32)))
                square_mine[n, :, cols] = jnp.sum(square.T, axis=0, keepdims=True)

        for shift in range(1, splits):
            small_square(shift).start()

    def grads_down():
        down_acc[...] = jnp.zeros_like(down_acc)

        @pl.loop(0, model_width // (2 * TILE))
        def _(tile):
            cols = pl.ds(pl.multiple_of(tile * 2 * TILE, LANES), 2 * TILE)
            right = rows[1, :, :, :, cols].reshape(GROUPS * span, 2 * TILE)
            grad = lax.dot_general(
                weighted[...], right, (((0,), (0,)), ((), ())), preferred_element_type=f32
            ).astype(bf16)
            down_out[:, cols] = grad
            down_acc[...] += lane_sums(jnp.square(grad.astype(f32)))

        down_square_out[...] = jnp.sum(down_acc[...].T, axis=0, keepdims=True)

    packed[0, 1, :, pl.ds(0, plan[1][1])] = pack(1, 0)
    packed[1, 1, :, pl.ds(0, plan[1][1])] = pack(1, 1)
    pl.semaphore_wait(barrier, experts - 1 + splits - 1)
    for i in (2, 0, 1):
        far_copy(1, i).start()
    for step in range(2, GROUPS):
        far_copy(step, 2).start()
        for i in range(2):
            packed[i, step, :, pl.ds(0, plan[step][1])] = pack(step, i)
            far_copy(step, i).start()
    for i in range(2):
        spread(0, i, pack(0, i))
    scale_in[0, seat] = scale_ref[me]
    for step in range(GROUPS):

        @pl.loop(0 if step else 1, members)
        def _(hop):
            scale_copy(step, hop).start()

    forward(0, 0)
    arrive(1, 0)
    forward(0, 1)
    arrive(1, 1)
    forward(1, 0)
    for load in weight_loads:
        load.wait()
    complete(0)
    compute(0)
    arrive(2, 0)
    forward(1, 1)
    arrive(2, 1)
    forward(2, 0)
    complete(1)
    compute(1)
    send_swaps(1)
    arrive(3, 0)
    forward(2, 1)
    arrive(3, 1)
    forward(3, 0)
    complete(2)
    compute(2)
    send_swaps(2)
    forward(3, 1)
    route_home(0)
    route_home(1)
    reduce(1)
    complete(3)
    compute(3)
    send_swaps(3)
    send_swaps(0)
    collect(1)
    grads_in()
    reduce(2)
    route_home(2)
    route_home(3)
    grads_down()
    collect(2)
    reduce(3)
    reduce(0)
    collect(3)
    collect(0)

    for shift in range(1, splits):
        small_square(shift).wait_recv()
    value = square_mine[...]
    for shift in range(1, splits):
        value = value + peer_square[shift - 1]
    square_out[...] = value
    for step in range(1, GROUPS):
        home_copy(step).wait_recv()
    everything = back[...].reshape(-1, width)
    selector = gsel_ref[...].reshape(everything.shape[0], -1)
    token_out[...] = lax.dot_general(
        selector, everything, (((0,), (0,)), ((), ())), preferred_element_type=f32
    ).astype(bf16)

    for step in range(GROUPS):
        if step:
            home_copy(step).wait_send()
            for i in range(3):
                far_copy(step, i).wait_send()

        @pl.loop(1, members)
        def _(hop):
            for i in range(2):
                near_copy(step, hop, i).wait_send()
            join_copy(step, hop).wait_send()

        @pl.loop(0, members)
        def _(hop):
            for shift in range(1, splits):
                swap(step, hop, shift).wait_send()

        @pl.loop(0 if step else 1, members)
        def _(hop):
            for shift in range(1, splits):
                for i in range(2):
                    relay(step, hop, shift, i, col).wait_send()
            scale_copy(step, hop).wait_send()
            route_copy(step, hop).wait()

        for shift in range(1, splits):
            small_route(step, shift).wait_send()
    for shift in range(1, splits):
        small_square(shift).wait_send()


def layer(tokens, cot, gsel, choice, scale, gate, up, down, experts, splits):
    members = experts // GROUPS
    tok_rows, model_width = tokens.shape
    group_cap, span = choice.shape[1:]
    capacity = span // members
    hidden_width = gate.shape[1]
    width = model_width // splits
    window = max(w for _, w in column_plan(model_width, splits))
    f32, bf16 = jnp.float32, jnp.bfloat16
    vmem = pl.BlockSpec(memory_space=pltpu.VMEM)
    hbm = pl.BlockSpec(memory_space=pl.ANY)
    dma = pltpu.SemaphoreType.DMA
    shape = jax.ShapeDtypeStruct
    slots = (GROUPS, members, capacity)
    return pl.pallas_call(
        functools.partial(layer_kernel, experts, splits),
        out_shape=(
            shape((tok_rows, width), bf16),
            shape((experts, 1, span), f32),
            shape((model_width, hidden_width), bf16),
            shape((model_width, hidden_width), bf16),
            shape((2, 1, model_width), f32),
            shape((hidden_width, model_width), bf16),
            shape((1, hidden_width), f32),
        ),
        in_specs=[vmem] * 5 + [hbm] * 3,
        out_specs=(vmem,) * 7,
        scratch_shapes=[
            pltpu.VMEM((2, GROUPS, group_cap, window), bf16),
            pltpu.VMEM((2, GROUPS, group_cap, window), bf16),
            pltpu.VMEM((GROUPS, group_cap, span), bf16),
            pltpu.VMEM((2,) + slots + (model_width,), bf16),
            pltpu.VMEM((2,) + slots + (model_width,), bf16),
            pltpu.VMEM((GROUPS, members, 1, LANES), f32),
            pltpu.VMEM((model_width, 2 * hidden_width), bf16),
            pltpu.VMEM((hidden_width, model_width), bf16),
            pltpu.VMEM((GROUPS * span, 2 * hidden_width), bf16),
            pltpu.VMEM((GROUPS * span, hidden_width), bf16),
            pltpu.VMEM(slots + (model_width,), bf16),
            pltpu.VMEM((splits - 1,) + slots + (width,), bf16),
            pltpu.VMEM(slots + (width,), bf16),
            pltpu.VMEM(slots + (width,), bf16),
            pltpu.VMEM((GROUPS, group_cap, width), bf16),
            pltpu.VMEM((GROUPS, group_cap, width), bf16),
            pltpu.VMEM((GROUPS, 1, span), f32),
            pltpu.VMEM((splits - 1, GROUPS, 1, span), f32),
            pltpu.VMEM((GROUPS, 1, span), f32),
            pltpu.VMEM((2, 1, model_width), f32),
            pltpu.VMEM((splits - 1, 2, 1, model_width), f32),
            pltpu.VMEM((hidden_width, LANES), f32),
            dma((3, GROUPS)), dma((3, GROUPS)),
            dma((2, GROUPS, members)), dma((2, GROUPS, members)),
            dma((2, splits - 1, GROUPS, members)), dma((2, splits - 1, GROUPS, members)),
            dma((GROUPS, members)), dma((GROUPS, members)),
            dma((splits - 1, GROUPS, members)), dma((splits - 1, GROUPS, members)),
            dma((GROUPS, members)), dma((GROUPS, members)),
            dma((GROUPS,)), dma((GROUPS,)),
            dma((splits - 1, GROUPS)), dma((splits - 1, GROUPS)),
            dma((GROUPS, members)), dma((GROUPS, members)),
            dma((splits - 1,)), dma((splits - 1,)),
            dma((3,)),
        ],
        compiler_params=pltpu.CompilerParams(
            collective_id=0, has_side_effects=True, vmem_limit_bytes=60000 * 1024
        ),
    )(tokens, cot, gsel, choice, scale, gate, up, down)


def on_device(tokens, expert_ids, route_weights, cotangent, w_gate, w_up, w_down):
    tok_rows, model_width = tokens.shape
    topk = expert_ids.shape[1]
    experts = lax.axis_size("ep")
    splits = lax.axis_size("tp")
    capacity = 2 * tok_rows * topk // experts
    slot_count = experts * capacity
    f32, bf16 = jnp.float32, jnp.bfloat16

    expert_iota = jnp.arange(experts, dtype=jnp.int32)[None, :]
    slots = jnp.arange(slot_count, dtype=jnp.int32)[None, :]
    slot_expert = slots // capacity
    spread = (expert_iota.reshape(experts, 1) == slot_expert).astype(bf16)
    picks = [expert_ids[:, k : k + 1] == expert_iota for k in range(topk)]
    member = sum(p.astype(f32) for p in picks)
    weight = sum(
        jnp.where(p, route_weights[:, k : k + 1].astype(f32), 0.0) for k, p in enumerate(picks)
    ).astype(bf16)
    order = jnp.arange(tok_rows, dtype=jnp.int32)
    earlier = (order[:, None] > order[None, :]).astype(bf16)
    before = jnp.dot(earlier, member.astype(bf16), preferred_element_type=f32)
    rank = jnp.where(member > 0, before, -1.0).astype(bf16)
    slot_rank = jnp.dot(rank, spread, preferred_element_type=f32)
    chosen = slot_rank == (slots % capacity).astype(f32)
    select = chosen.astype(bf16)
    slot_weight = jnp.sum(
        jnp.where(chosen, jnp.dot(weight, spread, preferred_element_type=f32), 0.0), axis=0
    )
    members = experts // GROUPS
    group_cap = members * capacity // topk
    group_slots = jnp.arange(GROUPS * group_cap, dtype=jnp.int32)[None, :]
    group_iota = jnp.arange(GROUPS, dtype=jnp.int32)[None, :]
    in_group = expert_ids[:, :1] // members == group_iota
    group_before = jnp.dot(earlier, in_group.astype(bf16), preferred_element_type=f32)
    own_rank = jnp.sum(jnp.where(in_group, group_before, 0.0), axis=1, keepdims=True).astype(jnp.int32)
    own_slot = expert_ids[:, :1] // members * group_cap + own_rank
    group_select = (own_slot == group_slots).astype(bf16)
    grouped = lax.dot_general(
        group_select, select, (((0,), (0,)), ((), ())), preferred_element_type=f32
    ).astype(bf16)
    span = members * capacity
    choice = jnp.stack(
        [
            grouped[g * group_cap : (g + 1) * group_cap, g * span : (g + 1) * span]
            for g in range(GROUPS)
        ]
    )
    gsel = group_select.T.reshape(GROUPS, group_cap, tok_rows)

    lane_pad = -capacity % LANES
    scale_out = jnp.pad(slot_weight.reshape(experts, 1, capacity), ((0, 0), (0, 0), (0, lane_pad)))
    token_grad, back_route, grad_gate, grad_up, squares, grad_down, down_square = layer(
        tokens, cotangent, gsel, choice, scale_out, w_gate[0], w_up[0], w_down[0], experts, splits
    )
    seat = lax.rem(lax.axis_index("ep"), members)
    slot_route = lax.dynamic_slice_in_dim(
        back_route.reshape(experts, members, capacity), seat, 1, 1
    ).reshape(1, slot_count)
    route_grad = jnp.concatenate(
        [
            jnp.sum(
                jnp.where(chosen & (slot_expert == expert_ids[:, k : k + 1]), slot_route, 0.0),
                axis=1, keepdims=True,
            )
            for k in range(topk)
        ],
        axis=1,
    ).astype(bf16)
    return (
        token_grad,
        route_grad,
        grad_gate[None],
        grad_up[None],
        grad_down[None],
        squares[0],
        squares[1],
        down_square,
    )


def solution(mesh):
    return jax.shard_map(
        on_device,
        mesh=mesh,
        in_specs=(
            P("ep", None),
            P("ep", None),
            P("ep", None),
            P("ep", None),
            P("ep", None, "tp"),
            P("ep", None, "tp"),
            P("ep", "tp", None),
        ),
        out_specs=(
            P("ep", "tp"),
            P("ep", None),
            P("ep", None, "tp"),
            P("ep", None, "tp"),
            P("ep", "tp", None),
            P("ep", None),
            P("ep", None),
            P("ep", "tp"),
        ),
        check_vma=False,
    )
```

time: 127 us -> 105 us (0.83)
  matrix products: 20.6 us -> 1.14 us
  Pallas kernels: 95.7 us -> 88.8 us
  local copies, waits for them, and re-layouts: 4.85 us -> 10.7 us
  other arithmetic: 4.39 us -> 2.85 us
    dot_general x11 -> x0, matrix products: 19.4 us -> none  [the longest x3 7.7 us: outer(): lax.dot_general(left, right, (((0,), (0,)), ((), ())), preferred_element_...]
    unnamed x16 -> x19, local copies, waits for them, and re-layouts: 1.1 us -> 8.66 us
    pallas_call x2 -> x1, Pallas kernels: 95.7 us -> 88.8 us  [layer(): pl.pallas_call(functools.partial(layer_kernel, experts, splits), out_shap...]
    slice x7 -> x0, local copies, waits for them, and re-layouts: 2.16 us -> none  [the longest x1 0.81 us: on_device(): scale_col = got_scale[:, 0, :capacity].reshape(slot_count, 1)]
where the time goes in v1:
time: 105 us; the launch traced here: 104 us
  Pallas kernels  88.8 us (85%)
  local copies, waits for them, and re-layouts  10.7 us (10%)
  other arithmetic  2.85 us (3%)
  matrix products  1.14 us (1%)
    pallas_call x1, Pallas kernels, layer(): pl.pallas_call(functools.partial(layer_kernel, experts, splits), out_shap...  88.8 us
    unnamed x19, local copies, waits for them, and re-layouts  8.66 us

profile of v1, /device:TPU:0, one launch (start us, length us, event | category | flops | bytes accessed | tf_op | source)
XLA Modules:
  0.0 104.3 jit_solution(6284650310053301289)
XLA Ops:
  0.6 0.0 copy-start.4
  0.7 0.6 copy-done.4
  1.3 0.0 copy-start.5
  1.3 0.7 copy-done.5
  2.0 0.1 fusion.2
  2.2 0.4 convolution_compare_fusion
  2.6 0.3 fusion
  2.9 0.1 reshape.102
  2.9 0.6 pad.4.scale_ref
  3.6 0.7 compare_convert_fusion.gsel_ref
  4.3 0.3 convolution_convert_fusion
  4.6 0.6 pad_maximum_fusion.choice_ref
  5.3 88.8 %shard_map.134 = (bf16[128,1024]{1,0:T(8,128)(2,1)}, f32[16,1,128]{2,1,0:T(1,128)}, bf16[2048,256]{1,0:T(8,128)(2,1)}, bf16[2048,256]{1,0:T(8,128)(2,1)}, f32[2,...) custom-call(bf16[128,2048]{1,0:T(8,128)(2,1)} %tokens_ref.1, bf16[128,2048]{1,0:T(8,128)(2,1)} %cot_ref.1, ...), custom_call_target="tpu_custom_call" | custom-call | tf_op jit(solution)/shard_map/pallas_call | solution.py:483
  94.1 0.0 copy-start.3
  94.1 0.0 copy-start.2
  94.1 0.5 broadcast.91
  94.7 0.2 copy-done.3
  94.8 0.7 reduce.7
  95.5 0.0 copy-done.2
  95.5 0.6 slice_bitcast_fusion.4
  96.1 0.1 reshape.103
  96.2 0.1 broadcast_in_dim.87
  96.3 0.3 select_reduce_fusion.1
  96.6 0.5 pad_maximum_fusion.1
  97.1 1.7 %copy.24 = bf16[128,1024]{1,0:T(8,128)(2,1)} copy(bf16[128,1024]{1,0:T(8,128)(2,1)} %get-tuple-element.45) | data formatting | bytes 524288
  98.8 2.4 %copy.25 = bf16[1,2048,256]{2,1,0:T(8,128)(2,1)} copy(bf16[1,2048,256]{2,1,0:T(8,128)(2,1)} %bitcast.44) | data formatting | bytes 2097152
  101.1 0.0 copy-done.1
  101.1 1.0 copy.26
  102.1 0.6 copy-done
  102.7 1.0 copy.27
  103.7 0.0 copy-done.6
  103.7 0.6 copy.28
  (10 shorter events, 0.1 us)
Async XLA Ops:
  0.6 0.7 copy-start.4
  1.3 0.7 copy-start.5
  94.1 0.7 copy-start.3
  94.1 1.4 %copy-start.2 = (f32[2,1,2048]{2,1,0:T(1,128)S(1)}, f32[2,1,2048]{2,1,0:T(1,128)}, u32[]{:S(2)}) copy-start(f32[2,1,2048]{2,1,0:T(1,128)} %get-tuple-element.20) | copy-start | bytes 49156
  98.8 2.4 %copy-start.1 = (bf16[2048,256]{1,0:T(8,128)(2,1)S(1)}, bf16[2048,256]{1,0:T(8,128)(2,1)}, u32[]{:S(2)}) copy-start(bf16[2048,256]{1,0:T(8,128)(2,1)} %get-tuple-element.18) | copy-start | bytes 3145732
  101.1 1.6 %copy-start = (bf16[256,2048]{1,0:T(8,128)(2,1)S(1)}, bf16[256,2048]{1,0:T(8,128)(2,1)}, u32[]{:S(2)}) copy-start(bf16[256,2048]{1,0:T(8,128)(2,1)} %get-tuple-element.19) | copy-start | bytes 3145732
  102.7 1.0 copy-start.6

commit v2 on v1

--- a/solution.py
+++ b/solution.py
@@ -11,7 +11,15 @@
 MESH = pl.DeviceIdType.MESH
 LANES = 128
 TILE = 256
-SHARED = (0, 4, 2, 2)
+SHARED = (0, 14, 0, 16)
+FIRST_COMPUTE = "compute2"
+PLAN = (
+    "far21 far20 far10 spread00 forward00 spread01 far11 far31",
+    "spread21 forward01 forward21 spread20 far30 spread10 forward20",
+    "spread11 forward10 compute2 spread31 forward11 compute0",
+    "spread30 forward31 compute1 reduce2 forward30 compute3",
+    "reduce0 reduce1 down collect2 reduce3 collect1 collect3 wide collect0",
+)
 GROUPS = 4
 
 
@@ -54,8 +62,8 @@
 
 def column_plan(model_width, splits):
     plan = []
-    for eighths in SHARED:
-        shared = model_width * eighths // 8 // (splits * LANES) * (splits * LANES) if splits == 2 else 0
+    for part in SHARED:
+        shared = model_width * part // 16 // (splits * LANES) * (splits * LANES) if splits == 2 else 0
         cut = (model_width - shared) // splits
         plan.append((cut, cut + shared))
     return plan
@@ -63,9 +71,9 @@
 
 def layer_kernel(
     experts, splits,
-    tokens_ref, cot_ref, gsel_ref, choice_ref, scale_ref, gate_hbm, up_hbm, down_hbm,
-    token_out, back_route, gate_out, up_out, square_out, down_out, down_square_out,
-    packed, landed, landed_choice, stage, rows, scale_in, wide, down, cots, weighted,
+    ids_ref, weight_ref, tokens_hbm, cot_hbm, gate_hbm, up_hbm, down_hbm,
+    token_out, route_out, gate_out, up_out, gate_square_out, up_square_out, down_out, down_square_out,
+    tokens_ref, cot_ref, gsel_ref, choice_ref, scale_ref, back_route, packed, landed, landed_choice, stage, rows, scale_in, wide, down, cots, weighted,
     part, peer_part, total, gathered, finished, back, route_mine, peer_route, route_total,
     square_mine, peer_square, down_acc,
     far_send, far_recv, near_send, near_recv, relay_send, relay_recv, scale_send, scale_recv,
@@ -93,7 +101,11 @@
         pltpu.make_async_copy(up_hbm, wide.at[:, pl.ds(hidden_width, hidden_width)], local.at[1]),
         pltpu.make_async_copy(down_hbm, down, local.at[2]),
     )
-    for load in weight_loads:
+    input_loads = (
+        pltpu.make_async_copy(tokens_hbm, tokens_ref, local.at[3]),
+        pltpu.make_async_copy(cot_hbm, cot_ref, local.at[4]),
+    )
+    for load in input_loads + weight_loads:
         load.start()
 
     def window(step):
@@ -124,9 +136,36 @@
     def scale_copy(step, hop):
         there = places[step] * members + around(hop)
         return remote(
-            scale_ref.at[there], scale_in.at[step, seat],
+            scale_ref.at[places[step]], scale_in.at[step, seat],
             scale_send.at[step, hop], scale_recv.at[step, hop], there, col,
         )
+
+    mate = seat + 1 - 2 * lax.rem(seat, 2)
+    chip = seat - lax.rem(seat, 2)
+
+    def mate_copy(i, hop):
+        return remote(
+            stage.at[i, 0, mate], rows.at[i, 0, seat], near_send.at[i, 0, hop], near_recv.at[i, 0, hop],
+            group * members + mate, col,
+        )
+
+    mate_out = lax.rem(mate - seat + members, members)
+    mate_in = lax.rem(seat - mate + members, members)
+
+    def each_hop(step, own, outgoing, act):
+        if step:
+            first = 0 if own else 1
+
+            @pl.loop(first, members)
+            def _(hop):
+                act(hop)
+        else:
+
+            @pl.loop(2, members)
+            def _(turn):
+                other = lax.rem(chip + turn, members)
+                gap = other - seat if outgoing else seat - other
+                act(lax.rem(gap + members, members))
 
     def near_copy(step, hop, i):
         if step == 0:
@@ -194,36 +233,45 @@
         value = lax.dot_general(choice, block, (((0,), (0,)), ((), ())), preferred_element_type=f32)
         wide_cut = block.shape[1]
         stage[i, step, :, :, pl.ds(0, wide_cut)] = value.astype(bf16).reshape(members, capacity, wide_cut)
-
-        @pl.loop(1, members)
-        def _(hop):
-            near_copy(step, hop, i).start()
+        if step == 0:
+            mate_copy(i, mate_out).start()
+        each_hop(step, False, True, lambda hop: near_copy(step, hop, i).start())
 
         cols = window(step) if step else pl.ds(0, wide_cut)
         rows[i, step, seat, :, cols] = stage[i, step, seat, :, pl.ds(0, wide_cut)]
         if step:
-            for shift in range(1, splits):
+            for shift in relays(step):
                 relay(step, 0, shift, i, col).start()
 
+    def relays(step):
+        return range(1, splits) if plan[step][0] else ()
+
+    choices = set()
+
     def arrive(step, i):
-        if i == 0:
+        if step not in choices:
+            choices.add(step)
             far_copy(step, 2).wait_recv()
         far_copy(step, i).wait_recv()
         spread(step, i, landed[i, step, :, pl.ds(0, plan[step][1])])
 
     def forward(step, i):
-        @pl.loop(1, members)
-        def _(hop):
+        def pass_on(hop):
             near_copy(step, hop, i).wait_recv()
-            for shift in range(1, splits):
+            for shift in relays(step):
                 relay(step, hop, shift, i, col).start()
 
+        each_hop(step, False, False, pass_on)
+        if step == 0:
+            mate_copy(i, mate_in).wait_recv()
+
     def complete(step):
-        @pl.loop(0 if step else 1, members)
-        def _(hop):
-            for shift in range(1, splits):
+        def landed_all(hop):
+            for shift in relays(step):
                 for i in range(2):
                     relay(step, hop, shift, i, lax.rem(col + splits - shift, splits)).wait_recv()
+
+        each_hop(step, True, False, landed_all)
 
         @pl.loop(0 if step else 1, members)
         def _(hop):
@@ -237,9 +285,9 @@
         hidden_back = lax.dot_general(
             slot_cot, down[...], (((1,), (1,)), ((), ())), preferred_element_type=f32
         )
-        spread_scale = jnp.broadcast_to(scale_in[step], (members, capacity, LANES))
-        lane = lax.broadcasted_iota(jnp.int32, (members, capacity, LANES), 2)
-        slot = lax.broadcasted_iota(jnp.int32, (members, capacity, LANES), 1)
+        spread_scale = jnp.broadcast_to(scale_in[step], (members, capacity, span))
+        lane = lax.broadcasted_iota(jnp.int32, (members, capacity, span), 2)
+        slot = lax.broadcasted_iota(jnp.int32, (members, capacity, span), 1) + seat * capacity
         scale = jnp.sum(jnp.where(lane == slot, spread_scale, 0.0), axis=2, keepdims=True)
         scale = scale.reshape(span, 1)
         gate_sig = jax.nn.sigmoid(gate_pre)
@@ -359,74 +407,122 @@
 
         down_square_out[...] = jnp.sum(down_acc[...].T, axis=0, keepdims=True)
 
-    packed[0, 1, :, pl.ds(0, plan[1][1])] = pack(1, 0)
-    packed[1, 1, :, pl.ds(0, plan[1][1])] = pack(1, 1)
-    pl.semaphore_wait(barrier, experts - 1 + splits - 1)
-    for i in (2, 0, 1):
-        far_copy(1, i).start()
-    for step in range(2, GROUPS):
-        far_copy(step, 2).start()
-        for i in range(2):
+    topk, tok_rows = ids_ref.shape
+    group_cap = gsel_ref.shape[1]
+
+    def count(shape, axis):
+        return lax.broadcasted_iota(jnp.int32, shape, axis).astype(f32)
+
+    def one_hot(mask):
+        return mask.astype(f32).astype(bf16)
+
+    ids = [ids_ref[pl.ds(k, 1), :].astype(f32) for k in range(topk)]
+    expert_count = count((experts, tok_rows), 0)
+    picks = [(expert_count == value).astype(f32) for value in ids]
+    named = sum(picks).astype(bf16)
+    earlier = one_hot(count((tok_rows, tok_rows), 0) < count((tok_rows, tok_rows), 1))
+    before_it = jnp.dot(named, earlier, preferred_element_type=f32)
+    ranks = [jnp.sum(pick * before_it, axis=0, keepdims=True) for pick in picks]
+    group_count = count((4 * GROUPS, tok_rows), 0) * members
+    in_group = ((ids[0] >= group_count) & (ids[0] < group_count + members)).astype(f32)
+    group_before = jnp.dot(in_group.astype(bf16), earlier, preferred_element_type=f32)
+    own_rank = jnp.sum(in_group * group_before, axis=0, keepdims=True)
+    for g in range(GROUPS):
+        inside = (count((group_cap, tok_rows), 0) == own_rank).astype(f32) * in_group[g : g + 1, :]
+        gsel_ref[g] = inside.astype(bf16)
+        slot_count = count((span, tok_rows), 0) + g * span
+        hits = [one_hot(slot_count == value * capacity + rank) for value, rank in zip(ids, ranks)]
+        choice_ref[g] = lax.dot_general(
+            inside.astype(bf16), sum(hits), (((1,), (1,)), ((), ())), preferred_element_type=f32
+        ).astype(bf16)
+        scales = sum(
+            lax.dot_general(
+                jnp.broadcast_to(weight_ref[pl.ds(k, 1), :].astype(f32), (16, tok_rows)).astype(bf16),
+                hits[k], (((1,), (1,)), ((), ())), preferred_element_type=f32,
+            )
+            for k in range(topk)
+        )
+        scale_ref[g] = scales[:1]
+
+    def route_back():
+        table = back_route[...].reshape(experts, span).astype(bf16)
+        lane = count((span, tok_rows), 0) - (seat * capacity).astype(f32)
+        for k in range(topk):
+            found = lax.dot_general(
+                table, picks[k].astype(bf16), (((0,), (0,)), ((), ())), preferred_element_type=f32
+            )
+            chosen = jnp.where(lane == ranks[k], found, 0.0)
+            route_out[pl.ds(k, 1), :] = jnp.sum(chosen, axis=0, keepdims=True).astype(bf16)
+
+    started = set()
+
+    def run(token):
+        name, digits = token.rstrip("0123456789"), token.lstrip("abcdefghijklmnopqrstuvwxyz")
+        step = int(digits[0]) if digits else 0
+        i = int(digits[1:]) if digits[1:] else 0
+        if name == "far":
             packed[i, step, :, pl.ds(0, plan[step][1])] = pack(step, i)
+            if not started:
+                pl.semaphore_wait(barrier, experts - 1 + splits - 1)
+            if step not in started:
+                started.add(step)
+                far_copy(step, 2).start()
             far_copy(step, i).start()
-    for i in range(2):
-        spread(0, i, pack(0, i))
-    scale_in[0, seat] = scale_ref[me]
+        elif name == "spread":
+            if step:
+                arrive(step, i)
+            else:
+                spread(step, i, pack(step, i))
+        elif name == "forward":
+            forward(step, i)
+        elif name == "compute":
+            complete(step)
+            compute(step)
+            send_swaps(step)
+        elif name == "reduce":
+            route_home(step)
+            reduce(step)
+        elif name == "collect":
+            collect(step)
+        elif name == "scale":
+            scale_in[0, seat] = scale_ref[group]
+            for n in range(GROUPS):
+
+                @pl.loop(0 if n else 1, members)
+                def _(hop):
+                    scale_copy(n, hop).start()
+        elif name == "load":
+            for load in weight_loads:
+                load.wait()
+        elif name == "wide":
+            grads_in()
+        else:
+            grads_down()
+
+    for load in input_loads:
+        load.wait()
+    for line in PLAN:
+        for token in line.split():
+            if token == "forward00":
+                run("scale")
+            if token == FIRST_COMPUTE:
+                run("load")
+            run(token)
+
     for step in range(GROUPS):
 
         @pl.loop(0 if step else 1, members)
         def _(hop):
-            scale_copy(step, hop).start()
-
-    forward(0, 0)
-    arrive(1, 0)
-    forward(0, 1)
-    arrive(1, 1)
-    forward(1, 0)
-    for load in weight_loads:
-        load.wait()
-    complete(0)
-    compute(0)
-    arrive(2, 0)
-    forward(1, 1)
-    arrive(2, 1)
-    forward(2, 0)
-    complete(1)
-    compute(1)
-    send_swaps(1)
-    arrive(3, 0)
-    forward(2, 1)
-    arrive(3, 1)
-    forward(3, 0)
-    complete(2)
-    compute(2)
-    send_swaps(2)
-    forward(3, 1)
-    route_home(0)
-    route_home(1)
-    reduce(1)
-    complete(3)
-    compute(3)
-    send_swaps(3)
-    send_swaps(0)
-    collect(1)
-    grads_in()
-    reduce(2)
-    route_home(2)
-    route_home(3)
-    grads_down()
-    collect(2)
-    reduce(3)
-    reduce(0)
-    collect(3)
-    collect(0)
-
+            route_copy(step, hop).wait_recv()
+
+    route_back()
     for shift in range(1, splits):
         small_square(shift).wait_recv()
     value = square_mine[...]
     for shift in range(1, splits):
         value = value + peer_square[shift - 1]
-    square_out[...] = value
+    gate_square_out[...] = value[0]
+    up_square_out[...] = value[1]
     for step in range(1, GROUPS):
         home_copy(step).wait_recv()
     everything = back[...].reshape(-1, width)
@@ -441,11 +537,21 @@
             for i in range(3):
                 far_copy(step, i).wait_send()
 
+        for i in range(2):
+            each_hop(step, False, True, lambda hop: near_copy(step, hop, i).wait_send())
+            if step == 0:
+                mate_copy(i, mate_out).wait_send()
+
         @pl.loop(1, members)
         def _(hop):
-            for i in range(2):
-                near_copy(step, hop, i).wait_send()
             join_copy(step, hop).wait_send()
+
+        def relays_sent(hop):
+            for shift in relays(step):
+                for i in range(2):
+                    relay(step, hop, shift, i, col).wait_send()
+
+        each_hop(step, True, False, relays_sent)
 
         @pl.loop(0, members)
         def _(hop):
@@ -454,11 +560,8 @@
 
         @pl.loop(0 if step else 1, members)
         def _(hop):
-            for shift in range(1, splits):
-                for i in range(2):
-                    relay(step, hop, shift, i, col).wait_send()
             scale_copy(step, hop).wait_send()
-            route_copy(step, hop).wait()
+            route_copy(step, hop).wait_send()
 
         for shift in range(1, splits):
             small_route(step, shift).wait_send()
@@ -466,17 +569,19 @@
         small_square(shift).wait_send()
 
 
-def layer(tokens, cot, gsel, choice, scale, gate, up, down, experts, splits):
+def layer(ids, weights, tokens, cot, gate, up, down, experts, splits):
     members = experts // GROUPS
-    tok_rows, model_width = tokens.shape
-    group_cap, span = choice.shape[1:]
-    capacity = span // members
+    topk, tok_rows = ids.shape
+    model_width = tokens.shape[1]
+    capacity = 2 * tok_rows * topk // experts
+    span = members * capacity
+    group_cap = span // topk
     hidden_width = gate.shape[1]
     width = model_width // splits
     window = max(w for _, w in column_plan(model_width, splits))
     f32, bf16 = jnp.float32, jnp.bfloat16
     vmem = pl.BlockSpec(memory_space=pltpu.VMEM)
-    hbm = pl.BlockSpec(memory_space=pl.ANY)
+    hbm = pl.BlockSpec(memory_space=pltpu.HBM)
     dma = pltpu.SemaphoreType.DMA
     shape = jax.ShapeDtypeStruct
     slots = (GROUPS, members, capacity)
@@ -484,22 +589,29 @@
         functools.partial(layer_kernel, experts, splits),
         out_shape=(
             shape((tok_rows, width), bf16),
-            shape((experts, 1, span), f32),
+            shape((topk, tok_rows), bf16),
             shape((model_width, hidden_width), bf16),
             shape((model_width, hidden_width), bf16),
-            shape((2, 1, model_width), f32),
+            shape((1, model_width), f32),
+            shape((1, model_width), f32),
             shape((hidden_width, model_width), bf16),
             shape((1, hidden_width), f32),
         ),
-        in_specs=[vmem] * 5 + [hbm] * 3,
-        out_specs=(vmem,) * 7,
+        in_specs=[vmem] * 2 + [hbm] * 5,
+        out_specs=(vmem,) * 8,
         scratch_shapes=[
+            pltpu.VMEM((tok_rows, model_width), bf16),
+            pltpu.VMEM((tok_rows, model_width), bf16),
+            pltpu.VMEM((GROUPS, group_cap, tok_rows), bf16),
+            pltpu.VMEM((GROUPS, group_cap, span), bf16),
+            pltpu.VMEM((GROUPS, 1, span), f32),
+            pltpu.VMEM((experts, 1, span), f32),
             pltpu.VMEM((2, GROUPS, group_cap, window), bf16),
             pltpu.VMEM((2, GROUPS, group_cap, window), bf16),
             pltpu.VMEM((GROUPS, group_cap, span), bf16),
             pltpu.VMEM((2,) + slots + (model_width,), bf16),
             pltpu.VMEM((2,) + slots + (model_width,), bf16),
-            pltpu.VMEM((GROUPS, members, 1, LANES), f32),
+            pltpu.VMEM((GROUPS, members, 1, span), f32),
             pltpu.VMEM((model_width, 2 * hidden_width), bf16),
             pltpu.VMEM((hidden_width, model_width), bf16),
             pltpu.VMEM((GROUPS * span, 2 * hidden_width), bf16),
@@ -526,90 +638,51 @@
             dma((splits - 1, GROUPS)), dma((splits - 1, GROUPS)),
             dma((GROUPS, members)), dma((GROUPS, members)),
             dma((splits - 1,)), dma((splits - 1,)),
-            dma((3,)),
+            dma((5,)),
         ],
         compiler_params=pltpu.CompilerParams(
-            collective_id=0, has_side_effects=True, vmem_limit_bytes=60000 * 1024
+            collective_id=0, has_side_effects=True, vmem_limit_bytes=50000 * 1024
         ),
-    )(tokens, cot, gsel, choice, scale, gate, up, down)
+    )(ids, weights, tokens, cot, gate, up, down)
+
+
+def export_kernel(*refs):
+    count = len(refs) // 2
+    copies = [
+        pltpu.make_async_copy(refs[n], refs[count + n], refs[-1].at[n]) for n in range(count)
+    ]
+    for copy in copies:
+        copy.start()
+    for copy in copies:
+        copy.wait()
+
+
+def export(arrays):
+    return pl.pallas_call(
+        export_kernel,
+        out_shape=tuple(jax.ShapeDtypeStruct(a.shape, a.dtype) for a in arrays),
+        in_specs=[pl.BlockSpec(memory_space=pltpu.VMEM)] * len(arrays),
+        out_specs=(pl.BlockSpec(memory_space=pltpu.HBM),) * len(arrays),
+        scratch_shapes=[pltpu.SemaphoreType.DMA((len(arrays),))],
+        compiler_params=pltpu.CompilerParams(vmem_limit_bytes=8000 * 1024),
+    )(*arrays)
 
 
 def on_device(tokens, expert_ids, route_weights, cotangent, w_gate, w_up, w_down):
-    tok_rows, model_width = tokens.shape
-    topk = expert_ids.shape[1]
     experts = lax.axis_size("ep")
     splits = lax.axis_size("tp")
-    capacity = 2 * tok_rows * topk // experts
-    slot_count = experts * capacity
-    f32, bf16 = jnp.float32, jnp.bfloat16
-
-    expert_iota = jnp.arange(experts, dtype=jnp.int32)[None, :]
-    slots = jnp.arange(slot_count, dtype=jnp.int32)[None, :]
-    slot_expert = slots // capacity
-    spread = (expert_iota.reshape(experts, 1) == slot_expert).astype(bf16)
-    picks = [expert_ids[:, k : k + 1] == expert_iota for k in range(topk)]
-    member = sum(p.astype(f32) for p in picks)
-    weight = sum(
-        jnp.where(p, route_weights[:, k : k + 1].astype(f32), 0.0) for k, p in enumerate(picks)
-    ).astype(bf16)
-    order = jnp.arange(tok_rows, dtype=jnp.int32)
-    earlier = (order[:, None] > order[None, :]).astype(bf16)
-    before = jnp.dot(earlier, member.astype(bf16), preferred_element_type=f32)
-    rank = jnp.where(member > 0, before, -1.0).astype(bf16)
-    slot_rank = jnp.dot(rank, spread, preferred_element_type=f32)
-    chosen = slot_rank == (slots % capacity).astype(f32)
-    select = chosen.astype(bf16)
-    slot_weight = jnp.sum(
-        jnp.where(chosen, jnp.dot(weight, spread, preferred_element_type=f32), 0.0), axis=0
+    results = layer(
+        expert_ids.T, route_weights.T, tokens, cotangent, w_gate[0], w_up[0], w_down[0], experts, splits
     )
-    members = experts // GROUPS
-    group_cap = members * capacity // topk
-    group_slots = jnp.arange(GROUPS * group_cap, dtype=jnp.int32)[None, :]
-    group_iota = jnp.arange(GROUPS, dtype=jnp.int32)[None, :]
-    in_group = expert_ids[:, :1] // members == group_iota
-    group_before = jnp.dot(earlier, in_group.astype(bf16), preferred_element_type=f32)
-    own_rank = jnp.sum(jnp.where(in_group, group_before, 0.0), axis=1, keepdims=True).astype(jnp.int32)
-    own_slot = expert_ids[:, :1] // members * group_cap + own_rank
-    group_select = (own_slot == group_slots).astype(bf16)
-    grouped = lax.dot_general(
-        group_select, select, (((0,), (0,)), ((), ())), preferred_element_type=f32
-    ).astype(bf16)
-    span = members * capacity
-    choice = jnp.stack(
-        [
-            grouped[g * group_cap : (g + 1) * group_cap, g * span : (g + 1) * span]
-            for g in range(GROUPS)
-        ]
-    )
-    gsel = group_select.T.reshape(GROUPS, group_cap, tok_rows)
-
-    lane_pad = -capacity % LANES
-    scale_out = jnp.pad(slot_weight.reshape(experts, 1, capacity), ((0, 0), (0, 0), (0, lane_pad)))
-    token_grad, back_route, grad_gate, grad_up, squares, grad_down, down_square = layer(
-        tokens, cotangent, gsel, choice, scale_out, w_gate[0], w_up[0], w_down[0], experts, splits
-    )
-    seat = lax.rem(lax.axis_index("ep"), members)
-    slot_route = lax.dynamic_slice_in_dim(
-        back_route.reshape(experts, members, capacity), seat, 1, 1
-    ).reshape(1, slot_count)
-    route_grad = jnp.concatenate(
-        [
-            jnp.sum(
-                jnp.where(chosen & (slot_expert == expert_ids[:, k : k + 1]), slot_route, 0.0),
-                axis=1, keepdims=True,
-            )
-            for k in range(topk)
-        ],
-        axis=1,
-    ).astype(bf16)
+    token_grad, route_grad, grad_gate, grad_up, gate_square, up_square, grad_down, down_square = export(results)
     return (
         token_grad,
-        route_grad,
+        route_grad.T,
         grad_gate[None],
         grad_up[None],
         grad_down[None],
-        squares[0],
-        squares[1],
+        gate_square,
+        up_square,
         down_square,
     )
 

time: 105 us -> 81.5 us (0.78)
  Pallas kernels: 88.8 us -> 77.8 us
  local copies, waits for them, and re-layouts: 10.7 us -> 2.75 us
  other arithmetic: 2.85 us -> 0 us
  matrix products: 1.14 us -> 0 us
    pallas_call x1, Pallas kernels: 88.8 us -> 76 us  [layer(): pl.pallas_call(functools.partial(layer_kernel, experts, splits), out_shap...]
    unnamed x19 -> x8, local copies, waits for them, and re-layouts: 8.66 us -> 2.75 us
    pallas_call x0 -> x1, Pallas kernels: none -> 1.83 us  [export(): pl.pallas_call(export_kernel, out_shape=tuple((jax.ShapeDtypeStruct(a.sha...]
    dot_general x4 -> x0, matrix products: 1.14 us -> none  [the longest x1 0.39 us: on_device(): slot_rank = jnp.dot(rank, spread, preferred_element_type=f32)]
where the time goes in v2:
time: 81.5 us; the launch traced here: 81.2 us
  Pallas kernels  77.8 us (95%)
  local copies, waits for them, and re-layouts  2.75 us (3%)
    pallas_call x1, Pallas kernels, layer(): pl.pallas_call(functools.partial(layer_kernel, experts, splits), out_shap...  76 us
    unnamed x8, local copies, waits for them, and re-layouts  2.75 us
    pallas_call x1, Pallas kernels, export(): pl.pallas_call(export_kernel, out_shape=tuple((jax.ShapeDtypeStruct(a.sha...  1.83 us

profile of v2, /device:TPU:0, one launch (start us, length us, event | category | flops | bytes accessed | tf_op | source)
XLA Modules:
  0.0 81.2 jit_solution(9371654024471306618)
XLA Ops:
  0.6 0.0 copy-start.2
  0.6 0.0 copy-start.3
  0.7 0.7 copy-done.2
  1.3 0.0 copy-done.3
  1.3 0.0 copy-start
  1.3 1.0 %copy-done = bf16[128,2048]{1,0:T(8,128)(2,1)S(1)} copy-done((bf16[128,2048]{1,0:T(8,128)(2,1)S(1)}, bf16[128,2048]{1,0:T(8,128)(2,1)}, u32[]{:S(2)}) %copy-start) | copy-done | bytes 524312
  2.4 0.0 copy-start.1
  2.4 1.0 %copy-done.1 = bf16[128,2048]{1,0:T(8,128)(2,1)S(1)} copy-done((bf16[128,2048]{1,0:T(8,128)(2,1)S(1)}, bf16[128,2048]{1,0:T(8,128)(2,1)}, u32[]{:S(2)}) %copy-start.1) | copy-done | bytes 524312
  3.4 76.0 %shard_map.134 = (bf16[128,1024]{1,0:T(8,128)(2,1)S(1)}, bf16[2,128]{1,0:T(2,128)(2,1)S(1)}, bf16[2048,256]{1,0:T(8,128)(2,1)S(1)}, bf16[2048,256]{1,0:T(8,128)(...) custom-call(s32[2,128]{1,0:T(2,128)S(1)} %bitcast.9, ...), custom_call_target="tpu_custom_call" | custom-call | tf_op jit(solution)/shard_map/pallas_call | solution.py:588
  79.4 1.8 %shard_map.135 = (bf16[128,1024]{1,0:T(8,128)(2,1)}, bf16[2,128]{1,0:T(2,128)(2,1)}, bf16[2048,256]{1,0:T(8,128)(2,1)}, bf16[2048,256]{1,0:T(8,128)(2,1)}, f32[1...) custom-call(bf16[128,1024]{1,0:T(8,128)(2,1)S(1)} %get-tuple-element.24.refs_0_, ...), custom_call_target="tpu_custom_call" | custom-call | tf_op jit(solution)/shard_map/pallas_call | solution.py:661
Async XLA Ops:
  0.6 0.7 copy-start.2
  0.6 0.7 copy-start.3
  1.3 1.0 %copy-start = (bf16[128,2048]{1,0:T(8,128)(2,1)S(1)}, bf16[128,2048]{1,0:T(8,128)(2,1)}, u32[]{:S(2)}) copy-start(bf16[128,2048]{1,0:T(8,128)(2,1)} %tokens_hbm.1) | copy-start | bytes 1572868
  2.4 1.0 %copy-start.1 = (bf16[128,2048]{1,0:T(8,128)(2,1)S(1)}, bf16[128,2048]{1,0:T(8,128)(2,1)}, u32[]{:S(2)}) copy-start(bf16[128,2048]{1,0:T(8,128)(2,1)} %cot_hbm.1) | copy-start | bytes 1572868

commit v3 on v2

--- a/solution.py
+++ b/solution.py
@@ -14,11 +14,11 @@
 SHARED = (0, 14, 0, 16)
 FIRST_COMPUTE = "compute2"
 PLAN = (
-    "far21 far20 far10 spread00 forward00 spread01 far11 far31",
-    "spread21 forward01 forward21 spread20 far30 spread10 forward20",
-    "spread11 forward10 compute2 spread31 forward11 compute0",
-    "spread30 forward31 compute1 reduce2 forward30 compute3",
-    "reduce0 reduce1 down collect2 reduce3 collect1 collect3 wide collect0",
+    "far21", "far20", "far10", "spread00", "forward00", "spread01", "far11", "far31", "spread21",
+    "forward01", "forward21", "spread20", "far30", "spread10", "forward20", "spread11", "forward10",
+    "compute2", "spread31", "forward11", "compute0", "spread30", "forward31", "compute1", "reduce2",
+    "forward30", "compute3", "reduce0", "reduce1", "down", "collect2", "reduce3", "collect1",
+    "collect3", "wide", "collect0",
 )
 GROUPS = 4
 
@@ -501,13 +501,12 @@
 
     for load in input_loads:
         load.wait()
-    for line in PLAN:
-        for token in line.split():
-            if token == "forward00":
-                run("scale")
-            if token == FIRST_COMPUTE:
-                run("load")
-            run(token)
+    for token in PLAN:
+        if token == "forward00":
+            run("scale")
+        if token == FIRST_COMPUTE:
+            run("load")
+        run(token)
 
     for step in range(GROUPS):
 
@@ -582,6 +581,9 @@
     f32, bf16 = jnp.float32, jnp.bfloat16
     vmem = pl.BlockSpec(memory_space=pltpu.VMEM)
     hbm = pl.BlockSpec(memory_space=pltpu.HBM)
+    tokens, cot, gate, up, down = (
+        pltpu.with_memory_space_constraint(v, pltpu.HBM) for v in (tokens, cot, gate, up, down)
+    )
     dma = pltpu.SemaphoreType.DMA
     shape = jax.ShapeDtypeStruct
     slots = (GROUPS, members, capacity)
@@ -641,7 +643,7 @@
             dma((5,)),
         ],
         compiler_params=pltpu.CompilerParams(
-            collective_id=0, has_side_effects=True, vmem_limit_bytes=50000 * 1024
+            collective_id=0, has_side_effects=True, vmem_limit_bytes=40000 * 1024
         ),
     )(ids, weights, tokens, cot, gate, up, down)
 

time: 81.5 us -> 76.7 us (0.941)
  Pallas kernels: 77.8 us -> 75 us
  local copies, waits for them, and re-layouts: 2.75 us -> 0.67 us
    pallas_call x1, Pallas kernels: 76 us -> 73.2 us  [layer(): pl.pallas_call(functools.partial(layer_kernel, experts, splits), out_shap...]
    unnamed x8 -> x4, local copies, waits for them, and re-layouts: 2.75 us -> 0.67 us
where the time goes in v3:
time: 76.7 us; the launch traced here: 76.3 us
  Pallas kernels  75 us (98%)
    pallas_call x1, Pallas kernels, layer(): pl.pallas_call(functools.partial(layer_kernel, experts, splits), out_shap...  73.2 us
    pallas_call x1, Pallas kernels, export(): pl.pallas_call(export_kernel, out_shape=tuple((jax.ShapeDtypeStruct(a.sha...  1.83 us

profile of v3, /device:TPU:0, one launch (start us, length us, event | category | flops | bytes accessed | tf_op | source)
XLA Modules:
  0.0 76.3 jit_solution(17300592318726985731)
XLA Ops:
  0.6 0.0 copy-start
  0.6 0.0 copy-start.1
  0.7 0.7 copy-done
  1.3 0.0 copy-done.1
  1.3 73.2 %shard_map.134 = (bf16[128,1024]{1,0:T(8,128)(2,1)S(1)}, bf16[2,128]{1,0:T(2,128)(2,1)S(1)}, bf16[2048,256]{1,0:T(8,128)(2,1)S(1)}, bf16[2048,256]{1,0:T(8,128)(...) custom-call(s32[2,128]{1,0:T(2,128)S(1)} %bitcast.9, ...), custom_call_target="tpu_custom_call" | custom-call | tf_op jit(solution)/shard_map/pallas_call | solution.py:590
  74.5 1.8 %shard_map.135 = (bf16[128,1024]{1,0:T(8,128)(2,1)}, bf16[2,128]{1,0:T(2,128)(2,1)}, bf16[2048,256]{1,0:T(8,128)(2,1)}, bf16[2048,256]{1,0:T(8,128)(2,1)}, f32[1...) custom-call(bf16[128,1024]{1,0:T(8,128)(2,1)S(1)} %get-tuple-element.24.refs_0_, ...), custom_call_target="tpu_custom_call" | custom-call | tf_op jit(solution)/shard_map/pallas_call | solution.py:663
Async XLA Ops:
  0.6 0.7 copy-start
  0.6 0.7 copy-start.1

commit v4 on v3

--- a/solution.py
+++ b/solution.py
@@ -11,16 +11,19 @@
 MESH = pl.DeviceIdType.MESH
 LANES = 128
 TILE = 256
-SHARED = (0, 14, 0, 16)
-FIRST_COMPUTE = "compute2"
+GROUPS = 4
+HALVES = 2
+WHOLE = ((0, 1, 0, 0), (1, 1, 1, 1), (0, 0, 0, 0), (1, 1, 0, 1))
 PLAN = (
-    "far21", "far20", "far10", "spread00", "forward00", "spread01", "far11", "far31", "spread21",
-    "forward01", "forward21", "spread20", "far30", "spread10", "forward20", "spread11", "forward10",
-    "compute2", "spread31", "forward11", "compute0", "spread30", "forward31", "compute1", "reduce2",
-    "forward30", "compute3", "reduce0", "reduce1", "down", "collect2", "reduce3", "collect1",
-    "collect3", "wide", "collect0",
+    "far11", "far23", "spread03", "far22", "far21", "spread01", "spread00", "spread02", "fwd03",
+    "far12", "spread23", "far20", "spread22", "far10", "fwd01", "far13", "far32", "fwd02", "spread11",
+    "fwd22", "far30", "fwd23", "far33", "spread21", "spread20", "fwd00", "spread12", "spread10",
+    "fwd20", "fwd21", "fwd11", "spread13", "comp00", "spread32", "comp20", "fwd13", "far31",
+    "fwd32", "spread30", "fwd10", "spread33", "fwd12", "comp10", "spread31", "red01", "fwd33",
+    "fwd30", "red20", "red21", "fwd31", "comp30", "red10", "grad10", "red00", "col20", "red11",
+    "col10", "col21", "red30", "grad30", "red31", "col00", "col30", "col31", "col11", "col01",
+    "grad20", "grad00",
 )
-GROUPS = 4
 
 
 def greet(experts, splits, me, col):
@@ -58,15 +61,6 @@
     if step == 2:
         return lax.rem(group + 2, GROUPS)
     return GROUPS - 1 - group
-
-
-def column_plan(model_width, splits):
-    plan = []
-    for part in SHARED:
-        shared = model_width * part // 16 // (splits * LANES) * (splits * LANES) if splits == 2 else 0
-        cut = (model_width - shared) // splits
-        plan.append((cut, cut + shared))
-    return plan
 
 
 def layer_kernel(
@@ -91,7 +85,10 @@
     hidden_width = down.shape[0]
     width = model_width // splits
     f32, bf16 = jnp.float32, jnp.bfloat16
-    plan = column_plan(model_width, splits)
+    halves = peer_part.shape[2]
+    half_width = width // halves
+    chunk = model_width // halves
+    chunks = range(2 * halves)
     places = [partner(group, step) for step in range(GROUPS)]
     barrier = greet(experts, splits, me, col)
     inputs = (tokens_ref, cot_ref)
@@ -108,13 +105,21 @@
     for load in input_loads + weight_loads:
         load.start()
 
-    def window(step):
-        cut, wide_cut = plan[step]
-        return pl.ds(pl.multiple_of(col * cut, LANES), wide_cut)
-
-    def relay_part(step, which):
-        cut, wide_cut = plan[step]
-        return pl.ds(pl.multiple_of(which * wide_cut, LANES), cut)
+    def whole(step, i):
+        return WHOLE[step][i * HALVES // halves]
+
+    def chunk_width(step, i):
+        return chunk if whole(step, i) else chunk // splits
+
+    def window(step, i):
+        base = i % halves * chunk
+        if whole(step, i):
+            return pl.ds(base, chunk)
+        return relay_part(step, i, col)
+
+    def relay_part(step, i, which):
+        cut = chunk // splits
+        return pl.ds(pl.multiple_of(i % halves * chunk + which * cut, LANES), cut)
 
     def around(hop):
         return lax.rem(seat + hop, members)
@@ -123,10 +128,10 @@
         return lax.rem(seat + members - hop, members)
 
     def far_copy(step, i):
-        if i == 2:
+        if i == 2 * halves:
             source, target = choice_ref.at[places[step]], landed_choice.at[step]
         else:
-            cols = pl.ds(0, plan[step][1])
+            cols = pl.ds(0, chunk_width(step, i))
             source, target = packed.at[i, step, :, cols], landed.at[i, step, :, cols]
         return remote(
             source, target, far_send.at[i, step], far_recv.at[i, step],
@@ -145,7 +150,7 @@
 
     def mate_copy(i, hop):
         return remote(
-            stage.at[i, 0, mate], rows.at[i, 0, seat], near_send.at[i, 0, hop], near_recv.at[i, 0, hop],
+            stage.at[i, 0, mate], rows.at[i // halves, 0, seat, :, pl.ds(i % halves * chunk, chunk)], near_send.at[i, 0, hop], near_recv.at[i, 0, hop],
             group * members + mate, col,
         )
 
@@ -168,28 +173,27 @@
                 act(lax.rem(gap + members, members))
 
     def near_copy(step, hop, i):
-        if step == 0:
-            source = stage.at[i, 0, around(hop), :, window(0)]
-        else:
-            source = stage.at[i, step, around(hop), :, pl.ds(0, plan[step][1])]
-        return remote(
-            source, rows.at[i, step, seat, :, window(step)],
+        size = chunk_width(step, i)
+        start = 0 if step or whole(step, i) else pl.multiple_of(col * size, LANES)
+        return remote(
+            stage.at[i, step, around(hop), :, pl.ds(start, size)],
+            rows.at[i // halves, step, seat, :, window(step, i)],
             near_send.at[i, step, hop], near_recv.at[i, step, hop], group * members + around(hop), col,
         )
 
     def relay(step, hop, shift, i, which):
-        block = rows.at[i, step, before(hop), :, relay_part(step, which)]
+        block = rows.at[i // halves, step, before(hop), :, relay_part(step, i, which)]
         return remote(
             block, block, relay_send.at[i, shift - 1, step, hop], relay_recv.at[i, shift - 1, step, hop],
             me, lax.rem(col + shift, splits),
         )
 
-    def swap(step, hop, shift):
+    def swap(step, b, hop, shift):
         peer = lax.rem(col + shift, splits)
-        theirs = pl.ds(pl.multiple_of(peer * width, LANES), width)
-        return remote(
-            part.at[step, around(hop), :, theirs], peer_part.at[shift - 1, step, around(hop)],
-            swap_send.at[shift - 1, step, hop], swap_recv.at[shift - 1, step, hop], me, peer,
+        theirs = pl.ds(pl.multiple_of(peer * width + b * half_width, LANES), half_width)
+        return remote(
+            part.at[step, around(hop), :, theirs], peer_part.at[shift - 1, step, b, around(hop)],
+            swap_send.at[shift - 1, step, b, hop], swap_recv.at[shift - 1, step, b, hop], me, peer,
         )
 
     def small_route(step, shift):
@@ -205,15 +209,15 @@
             me, lax.rem(col + shift, splits),
         )
 
-    def join_copy(step, hop):
-        return remote(
-            total.at[step, hop], gathered.at[step, seat],
-            join_send.at[step, hop], join_recv.at[step, hop], group * members + around(hop), col,
-        )
-
-    def home_copy(step):
-        return remote(
-            finished.at[step], back.at[group], home_send.at[step], home_recv.at[step],
+    def join_copy(step, b, hop):
+        return remote(
+            total.at[step, b, hop], gathered.at[step, b, seat],
+            join_send.at[step, b, hop], join_recv.at[step, b, hop], group * members + around(hop), col,
+        )
+
+    def home_copy(step, b):
+        return remote(
+            finished.at[step, b], back.at[b, group], home_send.at[step, b], home_recv.at[step, b],
             places[step] * members + seat, col,
         )
 
@@ -225,7 +229,8 @@
         )
 
     def pack(step, i):
-        source = inputs[i][:, window(step)] if step else inputs[i][...]
+        cols = window(step, i) if step else pl.ds(i % halves * chunk, chunk)
+        source = inputs[i // halves][:, cols]
         return jnp.dot(gsel_ref[places[step]], source, preferred_element_type=f32).astype(bf16)
 
     def spread(step, i, block):
@@ -237,28 +242,28 @@
             mate_copy(i, mate_out).start()
         each_hop(step, False, True, lambda hop: near_copy(step, hop, i).start())
 
-        cols = window(step) if step else pl.ds(0, wide_cut)
-        rows[i, step, seat, :, cols] = stage[i, step, seat, :, pl.ds(0, wide_cut)]
+        cols = window(step, i) if step else pl.ds(i % halves * chunk, chunk)
+        rows[i // halves, step, seat, :, cols] = stage[i, step, seat, :, pl.ds(0, wide_cut)]
         if step:
-            for shift in relays(step):
+            for shift in relays(step, i):
                 relay(step, 0, shift, i, col).start()
 
-    def relays(step):
-        return range(1, splits) if plan[step][0] else ()
+    def relays(step, i):
+        return () if whole(step, i) else range(1, splits)
 
     choices = set()
 
     def arrive(step, i):
         if step not in choices:
             choices.add(step)
-            far_copy(step, 2).wait_recv()
+            far_copy(step, 2 * halves).wait_recv()
         far_copy(step, i).wait_recv()
-        spread(step, i, landed[i, step, :, pl.ds(0, plan[step][1])])
+        spread(step, i, landed[i, step, :, pl.ds(0, chunk_width(step, i))])
 
     def forward(step, i):
         def pass_on(hop):
             near_copy(step, hop, i).wait_recv()
-            for shift in relays(step):
+            for shift in relays(step, i):
                 relay(step, hop, shift, i, col).start()
 
         each_hop(step, False, False, pass_on)
@@ -267,8 +272,8 @@
 
     def complete(step):
         def landed_all(hop):
-            for shift in relays(step):
-                for i in range(2):
+            for i in chunks:
+                for shift in relays(step, i):
                     relay(step, hop, shift, i, lax.rem(col + splits - shift, splits)).wait_recv()
 
         each_hop(step, True, False, landed_all)
@@ -319,10 +324,12 @@
             small_route(step, shift).start()
 
     def send_swaps(step):
-        @pl.loop(1, members + 1)
-        def _(turn):
-            for shift in range(1, splits):
-                swap(step, lax.rem(turn, members), shift).start()
+        for b in range(halves):
+
+            @pl.loop(1, members + 1)
+            def _(turn):
+                for shift in range(1, splits):
+                    swap(step, b, lax.rem(turn, members), shift).start()
 
     def route_home(step):
         value = route_mine[step]
@@ -337,37 +344,37 @@
         def _(hop):
             route_copy(step, hop).start()
 
-    def block_total(step, hop):
+    def block_total(step, b, hop):
         source = around(hop)
         for shift in range(1, splits):
-            swap(step, hop, shift).wait_recv()
-        mine = pl.ds(pl.multiple_of(col * width, LANES), width)
+            swap(step, b, hop, shift).wait_recv()
+        mine = pl.ds(pl.multiple_of(col * width + b * half_width, LANES), half_width)
         value = part[step, source, :, mine].astype(f32)
         for shift in range(1, splits):
-            value = value + peer_part[shift - 1, step, source].astype(f32)
+            value = value + peer_part[shift - 1, step, b, source].astype(f32)
         return value.astype(bf16)
 
-    def reduce(step):
+    def reduce(step, b):
         @pl.loop(1, members)
         def _(hop):
-            total[step, hop] = block_total(step, hop)
-            join_copy(step, hop).start()
-
-        gathered[step, seat] = block_total(step, 0)
-
-    def collect(step):
+            total[step, b, hop] = block_total(step, b, hop)
+            join_copy(step, b, hop).start()
+
+        gathered[step, b, seat] = block_total(step, b, 0)
+
+    def collect(step, b):
         @pl.loop(1, members)
         def _(hop):
-            join_copy(step, hop).wait_recv()
-
-        pairs = gathered[step].reshape(span, width)
+            join_copy(step, b, hop).wait_recv()
+
+        pairs = gathered[step, b].reshape(span, half_width)
         choice = landed_choice[step] if step else choice_ref[group]
         summed = jnp.dot(choice, pairs, preferred_element_type=f32).astype(bf16)
         if step:
-            finished[step] = summed
-            home_copy(step).start()
+            finished[step, b] = summed
+            home_copy(step, b).start()
         else:
-            back[group] = summed
+            back[b, group] = summed
 
     def lane_sums(value):
         folded = value[:, :LANES]
@@ -375,8 +382,10 @@
             folded = folded + value[:, start : start + LANES]
         return folded
 
-    def grads_in():
-        @pl.loop(0, model_width // TILE)
+    def grads_in(first):
+        tiles = model_width // TILE // 2
+
+        @pl.loop(first * tiles, (first + 1) * tiles)
         def _(tile):
             cols = pl.ds(pl.multiple_of(tile * TILE, LANES), TILE)
             left = rows[0, :, :, :, cols].reshape(GROUPS * span, TILE)
@@ -389,13 +398,10 @@
                 square = lane_sums(jnp.square(value.astype(f32)))
                 square_mine[n, :, cols] = jnp.sum(square.T, axis=0, keepdims=True)
 
-        for shift in range(1, splits):
-            small_square(shift).start()
-
-    def grads_down():
-        down_acc[...] = jnp.zeros_like(down_acc)
-
-        @pl.loop(0, model_width // (2 * TILE))
+    def grads_down(first):
+        tiles = model_width // TILE // 4
+
+        @pl.loop(first * tiles, (first + 1) * tiles)
         def _(tile):
             cols = pl.ds(pl.multiple_of(tile * 2 * TILE, LANES), 2 * TILE)
             right = rows[1, :, :, :, cols].reshape(GROUPS * span, 2 * TILE)
@@ -404,8 +410,6 @@
             ).astype(bf16)
             down_out[:, cols] = grad
             down_acc[...] += lane_sums(jnp.square(grad.astype(f32)))
-
-        down_square_out[...] = jnp.sum(down_acc[...].T, axis=0, keepdims=True)
 
     topk, tok_rows = ids_ref.shape
     group_cap = gsel_ref.shape[1]
@@ -430,10 +434,12 @@
     for g in range(GROUPS):
         inside = (count((group_cap, tok_rows), 0) == own_rank).astype(f32) * in_group[g : g + 1, :]
         gsel_ref[g] = inside.astype(bf16)
+
+    def make_choice(g):
         slot_count = count((span, tok_rows), 0) + g * span
         hits = [one_hot(slot_count == value * capacity + rank) for value, rank in zip(ids, ranks)]
         choice_ref[g] = lax.dot_general(
-            inside.astype(bf16), sum(hits), (((1,), (1,)), ((), ())), preferred_element_type=f32
+            gsel_ref[g], sum(hits), (((1,), (1,)), ((), ())), preferred_element_type=f32
         ).astype(bf16)
         scales = sum(
             lax.dot_general(
@@ -454,58 +460,76 @@
             chosen = jnp.where(lane == ranks[k], found, 0.0)
             route_out[pl.ds(k, 1), :] = jnp.sum(chosen, axis=0, keepdims=True).astype(bf16)
 
-    started = set()
+    down_acc[...] = jnp.zeros_like(down_acc)
+    begun = set()
+    grad_parts = [0, 0]
+
+    def first_time(name):
+        fresh = name not in begun
+        begun.add(name)
+        return fresh
+
+    def send_scales():
+        scale_in[0, seat] = scale_ref[group]
+        for step in range(GROUPS):
+
+            @pl.loop(0 if step else 1, members)
+            def _(hop):
+                scale_copy(step, hop).start()
 
     def run(token):
-        name, digits = token.rstrip("0123456789"), token.lstrip("abcdefghijklmnopqrstuvwxyz")
-        step = int(digits[0]) if digits else 0
-        i = int(digits[1:]) if digits[1:] else 0
+        name, step, i = token[:-2], int(token[-2]), int(token[-1])
+        if halves < HALVES and name != "comp" and name != "grad":
+            if i % HALVES:
+                return
+            i = i // HALVES
         if name == "far":
-            packed[i, step, :, pl.ds(0, plan[step][1])] = pack(step, i)
-            if not started:
+            packed[i, step, :, pl.ds(0, chunk_width(step, i))] = pack(step, i)
+            if first_time("far"):
                 pl.semaphore_wait(barrier, experts - 1 + splits - 1)
-            if step not in started:
-                started.add(step)
-                far_copy(step, 2).start()
             far_copy(step, i).start()
         elif name == "spread":
+            if first_time("spread"):
+                for g in range(GROUPS):
+                    make_choice(g)
+                for other in range(1, GROUPS):
+                    far_copy(other, 2 * halves).start()
             if step:
                 arrive(step, i)
             else:
                 spread(step, i, pack(step, i))
-        elif name == "forward":
+        elif name == "fwd":
+            if first_time("fwd"):
+                send_scales()
             forward(step, i)
-        elif name == "compute":
+        elif name == "comp":
+            if first_time("comp"):
+                for load in weight_loads:
+                    load.wait()
             complete(step)
             compute(step)
             send_swaps(step)
-        elif name == "reduce":
-            route_home(step)
-            reduce(step)
-        elif name == "collect":
-            collect(step)
-        elif name == "scale":
-            scale_in[0, seat] = scale_ref[group]
-            for n in range(GROUPS):
-
-                @pl.loop(0 if n else 1, members)
-                def _(hop):
-                    scale_copy(n, hop).start()
-        elif name == "load":
-            for load in weight_loads:
-                load.wait()
-        elif name == "wide":
-            grads_in()
+        elif name == "red":
+            if first_time("route%d" % step):
+                route_home(step)
+            reduce(step, i)
+        elif name == "col":
+            collect(step, i)
+        elif step < 2:
+            grads_in(grad_parts[0])
+            grad_parts[0] += 1
+            if grad_parts[0] == 2:
+                for shift in range(1, splits):
+                    small_square(shift).start()
         else:
-            grads_down()
+            grads_down(grad_parts[1])
+            grad_parts[1] += 1
+            if grad_parts[1] == 2:
+                down_square_out[...] = jnp.sum(down_acc[...].T, axis=0, keepdims=True)
 
     for load in input_loads:
         load.wait()
     for token in PLAN:
-        if token == "forward00":
-            run("scale")
-        if token == FIRST_COMPUTE:
-            run("load")
         run(token)
 
     for step in range(GROUPS):
@@ -522,32 +546,35 @@
         value = value + peer_square[shift - 1]
     gate_square_out[...] = value[0]
     up_square_out[...] = value[1]
-    for step in range(1, GROUPS):
-        home_copy(step).wait_recv()
-    everything = back[...].reshape(-1, width)
-    selector = gsel_ref[...].reshape(everything.shape[0], -1)
-    token_out[...] = lax.dot_general(
-        selector, everything, (((0,), (0,)), ((), ())), preferred_element_type=f32
-    ).astype(bf16)
+    selector = gsel_ref[...].reshape(GROUPS * group_cap, tok_rows)
+    for b in range(halves):
+        for step in range(1, GROUPS):
+            home_copy(step, b).wait_recv()
+        token_out[:, pl.ds(b * half_width, half_width)] = lax.dot_general(
+            selector, back[b].reshape(GROUPS * group_cap, half_width), (((0,), (0,)), ((), ())),
+            preferred_element_type=f32,
+        ).astype(bf16)
 
     for step in range(GROUPS):
         if step:
-            home_copy(step).wait_send()
-            for i in range(3):
+            for b in range(halves):
+                home_copy(step, b).wait_send()
+            for i in range(2 * halves + 1):
                 far_copy(step, i).wait_send()
 
-        for i in range(2):
+        for i in chunks:
             each_hop(step, False, True, lambda hop: near_copy(step, hop, i).wait_send())
             if step == 0:
                 mate_copy(i, mate_out).wait_send()
 
         @pl.loop(1, members)
         def _(hop):
-            join_copy(step, hop).wait_send()
+            for b in range(halves):
+                join_copy(step, b, hop).wait_send()
 
         def relays_sent(hop):
-            for shift in relays(step):
-                for i in range(2):
+            for i in chunks:
+                for shift in relays(step, i):
                     relay(step, hop, shift, i, col).wait_send()
 
         each_hop(step, True, False, relays_sent)
@@ -555,7 +582,8 @@
         @pl.loop(0, members)
         def _(hop):
             for shift in range(1, splits):
-                swap(step, hop, shift).wait_send()
+                for b in range(halves):
+                    swap(step, b, hop, shift).wait_send()
 
         @pl.loop(0 if step else 1, members)
         def _(hop):
@@ -577,7 +605,8 @@
     group_cap = span // topk
     hidden_width = gate.shape[1]
     width = model_width // splits
-    window = max(w for _, w in column_plan(model_width, splits))
+    halves = HALVES if experts * splits <= 64 else 1
+    half_width, chunk, chunks = width // halves, model_width // halves, 2 * halves
     f32, bf16 = jnp.float32, jnp.bfloat16
     vmem = pl.BlockSpec(memory_space=pltpu.VMEM)
     hbm = pl.BlockSpec(memory_space=pltpu.HBM)
@@ -608,10 +637,10 @@
             pltpu.VMEM((GROUPS, group_cap, span), bf16),
             pltpu.VMEM((GROUPS, 1, span), f32),
             pltpu.VMEM((experts, 1, span), f32),
-            pltpu.VMEM((2, GROUPS, group_cap, window), bf16),
-            pltpu.VMEM((2, GROUPS, group_cap, window), bf16),
+            pltpu.VMEM((chunks, GROUPS, group_cap, chunk), bf16),
+            pltpu.VMEM((chunks, GROUPS, group_cap, chunk), bf16),
             pltpu.VMEM((GROUPS, group_cap, span), bf16),
-            pltpu.VMEM((2,) + slots + (model_width,), bf16),
+            pltpu.VMEM((chunks,) + slots + (chunk,), bf16),
             pltpu.VMEM((2,) + slots + (model_width,), bf16),
             pltpu.VMEM((GROUPS, members, 1, span), f32),
             pltpu.VMEM((model_width, 2 * hidden_width), bf16),
@@ -619,24 +648,24 @@
             pltpu.VMEM((GROUPS * span, 2 * hidden_width), bf16),
             pltpu.VMEM((GROUPS * span, hidden_width), bf16),
             pltpu.VMEM(slots + (model_width,), bf16),
-            pltpu.VMEM((splits - 1,) + slots + (width,), bf16),
-            pltpu.VMEM(slots + (width,), bf16),
-            pltpu.VMEM(slots + (width,), bf16),
-            pltpu.VMEM((GROUPS, group_cap, width), bf16),
-            pltpu.VMEM((GROUPS, group_cap, width), bf16),
+            pltpu.VMEM((splits - 1, GROUPS, halves) + slots[1:] + (half_width,), bf16),
+            pltpu.VMEM((GROUPS, halves) + slots[1:] + (half_width,), bf16),
+            pltpu.VMEM((GROUPS, halves) + slots[1:] + (half_width,), bf16),
+            pltpu.VMEM((GROUPS, halves, group_cap, half_width), bf16),
+            pltpu.VMEM((halves, GROUPS, group_cap, half_width), bf16),
             pltpu.VMEM((GROUPS, 1, span), f32),
             pltpu.VMEM((splits - 1, GROUPS, 1, span), f32),
             pltpu.VMEM((GROUPS, 1, span), f32),
             pltpu.VMEM((2, 1, model_width), f32),
             pltpu.VMEM((splits - 1, 2, 1, model_width), f32),
             pltpu.VMEM((hidden_width, LANES), f32),
-            dma((3, GROUPS)), dma((3, GROUPS)),
-            dma((2, GROUPS, members)), dma((2, GROUPS, members)),
-            dma((2, splits - 1, GROUPS, members)), dma((2, splits - 1, GROUPS, members)),
+            dma((chunks + 1, GROUPS)), dma((chunks + 1, GROUPS)),
+            dma((chunks, GROUPS, members)), dma((chunks, GROUPS, members)),
+            dma((chunks, splits - 1, GROUPS, members)), dma((chunks, splits - 1, GROUPS, members)),
             dma((GROUPS, members)), dma((GROUPS, members)),
-            dma((splits - 1, GROUPS, members)), dma((splits - 1, GROUPS, members)),
-            dma((GROUPS, members)), dma((GROUPS, members)),
-            dma((GROUPS,)), dma((GROUPS,)),
+            dma((splits - 1, GROUPS, halves, members)), dma((splits - 1, GROUPS, halves, members)),
+            dma((GROUPS, halves, members)), dma((GROUPS, halves, members)),
+            dma((GROUPS, halves)), dma((GROUPS, halves)),
             dma((splits - 1, GROUPS)), dma((splits - 1, GROUPS)),
             dma((GROUPS, members)), dma((GROUPS, members)),
             dma((splits - 1,)), dma((splits - 1,)),

time: 76.7 us -> 75.2 us (0.980)
  Pallas kernels: 75 us -> 73.7 us
    pallas_call x1, Pallas kernels: 73.2 us -> 71.9 us  [layer(): pl.pallas_call(functools.partial(layer_kernel, experts, splits), out_shap...]
where the time goes in v4:
time: 75.2 us; the launch traced here: 75 us
  Pallas kernels  73.7 us (98%)
    pallas_call x1, Pallas kernels, layer(): pl.pallas_call(functools.partial(layer_kernel, experts, splits), out_shap...  71.9 us
    pallas_call x1, Pallas kernels, export(): pl.pallas_call(export_kernel, out_shape=tuple((jax.ShapeDtypeStruct(a.sha...  1.83 us

profile of v4, /device:TPU:0, one launch (start us, length us, event | category | flops | bytes accessed | tf_op | source)
XLA Modules:
  0.0 75.0 jit_solution(679966268035172485)
XLA Ops:
  0.6 0.0 copy-start
  0.6 0.0 copy-start.1
  0.7 0.7 copy-done
  1.3 0.0 copy-done.1
  1.3 71.9 %shard_map.134 = (bf16[128,1024]{1,0:T(8,128)(2,1)S(1)}, bf16[2,128]{1,0:T(2,128)(2,1)S(1)}, bf16[2048,256]{1,0:T(8,128)(2,1)S(1)}, bf16[2048,256]{1,0:T(8,128)(...) custom-call(s32[2,128]{1,0:T(2,128)S(1)} %bitcast.9, ...), custom_call_target="tpu_custom_call" | custom-call | tf_op jit(solution)/shard_map/pallas_call | solution.py:619
  73.2 1.8 %shard_map.135 = (bf16[128,1024]{1,0:T(8,128)(2,1)}, bf16[2,128]{1,0:T(2,128)(2,1)}, bf16[2048,256]{1,0:T(8,128)(2,1)}, bf16[2048,256]{1,0:T(8,128)(2,1)}, f32[1...) custom-call(bf16[128,1024]{1,0:T(8,128)(2,1)S(1)} %get-tuple-element.24.refs_0_, ...), custom_call_target="tpu_custom_call" | custom-call | tf_op jit(solution)/shard_map/pallas_call | solution.py:692
Async XLA Ops:
  0.6 0.7 copy-start
  0.6 0.7 copy-start.1

commit v5 on v4

--- a/solution.py
+++ b/solution.py
@@ -13,7 +13,7 @@
 TILE = 256
 GROUPS = 4
 HALVES = 2
-WHOLE = ((0, 1, 0, 0), (1, 1, 1, 1), (0, 0, 0, 0), (1, 1, 0, 1))
+WHOLE = ((0, 1, 0, 0), (1, 1, 1, 1), (0, 0, 0, 0), (1, 1, 1, 1))
 PLAN = (
     "far11", "far23", "spread03", "far22", "far21", "spread01", "spread00", "spread02", "fwd03",
     "far12", "spread23", "far20", "spread22", "far10", "fwd01", "far13", "far32", "fwd02", "spread11",
@@ -65,9 +65,9 @@
 
 def layer_kernel(
     experts, splits,
-    ids_ref, weight_ref, tokens_hbm, cot_hbm, gate_hbm, up_hbm, down_hbm,
+    ids_hbm, weight_hbm, tokens_hbm, cot_hbm, gate_hbm, up_hbm, down_hbm,
     token_out, route_out, gate_out, up_out, gate_square_out, up_square_out, down_out, down_square_out,
-    tokens_ref, cot_ref, gsel_ref, choice_ref, scale_ref, back_route, packed, landed, landed_choice, stage, rows, scale_in, wide, down, cots, weighted,
+    ids_ref, weight_ref, tokens_ref, cot_ref, gsel_ref, choice_ref, scale_ref, back_route, packed, landed, landed_choice, stage, rows, scale_in, wide, down, cots, weighted,
     part, peer_part, total, gathered, finished, back, route_mine, peer_route, route_total,
     square_mine, peer_square, down_acc,
     far_send, far_recv, near_send, near_recv, relay_send, relay_recv, scale_send, scale_recv,
@@ -102,7 +102,11 @@
         pltpu.make_async_copy(tokens_hbm, tokens_ref, local.at[3]),
         pltpu.make_async_copy(cot_hbm, cot_ref, local.at[4]),
     )
-    for load in input_loads + weight_loads:
+    route_loads = (
+        pltpu.make_async_copy(ids_hbm, ids_ref, local.at[5]),
+        pltpu.make_async_copy(weight_hbm, weight_ref, local.at[6]),
+    )
+    for load in route_loads + input_loads + weight_loads:
         load.start()
 
     def whole(step, i):
@@ -188,12 +192,12 @@
             me, lax.rem(col + shift, splits),
         )
 
-    def swap(step, b, hop, shift):
+    def swap(step, b, shift):
         peer = lax.rem(col + shift, splits)
         theirs = pl.ds(pl.multiple_of(peer * width + b * half_width, LANES), half_width)
         return remote(
-            part.at[step, around(hop), :, theirs], peer_part.at[shift - 1, step, b, around(hop)],
-            swap_send.at[shift - 1, step, b, hop], swap_recv.at[shift - 1, step, b, hop], me, peer,
+            part.at[step, :, :, theirs], peer_part.at[shift - 1, step, b],
+            swap_send.at[shift - 1, step, b], swap_recv.at[shift - 1, step, b], me, peer,
         )
 
     def small_route(step, shift):
@@ -325,11 +329,8 @@
 
     def send_swaps(step):
         for b in range(halves):
-
-            @pl.loop(1, members + 1)
-            def _(turn):
-                for shift in range(1, splits):
-                    swap(step, b, lax.rem(turn, members), shift).start()
+            for shift in range(1, splits):
+                swap(step, b, shift).start()
 
     def route_home(step):
         value = route_mine[step]
@@ -346,8 +347,6 @@
 
     def block_total(step, b, hop):
         source = around(hop)
-        for shift in range(1, splits):
-            swap(step, b, hop, shift).wait_recv()
         mine = pl.ds(pl.multiple_of(col * width + b * half_width, LANES), half_width)
         value = part[step, source, :, mine].astype(f32)
         for shift in range(1, splits):
@@ -355,6 +354,9 @@
         return value.astype(bf16)
 
     def reduce(step, b):
+        for shift in range(1, splits):
+            swap(step, b, shift).wait_recv()
+
         @pl.loop(1, members)
         def _(hop):
             total[step, b, hop] = block_total(step, b, hop)
@@ -411,6 +413,8 @@
             down_out[:, cols] = grad
             down_acc[...] += lane_sums(jnp.square(grad.astype(f32)))
 
+    for load in route_loads:
+        load.wait()
     topk, tok_rows = ids_ref.shape
     group_cap = gsel_ref.shape[1]
 
@@ -579,11 +583,9 @@
 
         each_hop(step, True, False, relays_sent)
 
-        @pl.loop(0, members)
-        def _(hop):
-            for shift in range(1, splits):
-                for b in range(halves):
-                    swap(step, b, hop, shift).wait_send()
+        for shift in range(1, splits):
+            for b in range(halves):
+                swap(step, b, shift).wait_send()
 
         @pl.loop(0 if step else 1, members)
         def _(hop):
@@ -610,8 +612,9 @@
     f32, bf16 = jnp.float32, jnp.bfloat16
     vmem = pl.BlockSpec(memory_space=pltpu.VMEM)
     hbm = pl.BlockSpec(memory_space=pltpu.HBM)
-    tokens, cot, gate, up, down = (
-        pltpu.with_memory_space_constraint(v, pltpu.HBM) for v in (tokens, cot, gate, up, down)
+    ids, weights, tokens, cot, gate, up, down = (
+        pltpu.with_memory_space_constraint(v, pltpu.HBM)
+        for v in (ids, weights, tokens, cot, gate, up, down)
     )
     dma = pltpu.SemaphoreType.DMA
     shape = jax.ShapeDtypeStruct
@@ -628,9 +631,11 @@
             shape((hidden_width, model_width), bf16),
             shape((1, hidden_width), f32),
         ),
-        in_specs=[vmem] * 2 + [hbm] * 5,
+        in_specs=[hbm] * 7,
         out_specs=(vmem,) * 8,
         scratch_shapes=[
+            pltpu.VMEM((topk, tok_rows), jnp.int32),
+            pltpu.VMEM((topk, tok_rows), bf16),
             pltpu.VMEM((tok_rows, model_width), bf16),
             pltpu.VMEM((tok_rows, model_width), bf16),
             pltpu.VMEM((GROUPS, group_cap, tok_rows), bf16),
@@ -663,13 +668,13 @@
             dma((chunks, GROUPS, members)), dma((chunks, GROUPS, members)),
             dma((chunks, splits - 1, GROUPS, members)), dma((chunks, splits - 1, GROUPS, members)),
             dma((GROUPS, members)), dma((GROUPS, members)),
-            dma((splits - 1, GROUPS, halves, members)), dma((splits - 1, GROUPS, halves, members)),
+            dma((splits - 1, GROUPS, halves)), dma((splits - 1, GROUPS, halves)),
             dma((GROUPS, halves, members)), dma((GROUPS, halves, members)),
             dma((GROUPS, halves)), dma((GROUPS, halves)),
             dma((splits - 1, GROUPS)), dma((splits - 1, GROUPS)),
             dma((GROUPS, members)), dma((GROUPS, members)),
             dma((splits - 1,)), dma((splits - 1,)),
-            dma((5,)),
+            dma((7,)),
         ],
         compiler_params=pltpu.CompilerParams(
             collective_id=0, has_side_effects=True, vmem_limit_bytes=40000 * 1024

time: 75.2 us -> 73.7 us (0.980)
  Pallas kernels: 73.7 us -> 72.9 us
    pallas_call x1, Pallas kernels: 71.9 us -> 71.1 us  [layer(): pl.pallas_call(functools.partial(layer_kernel, experts, splits), out_shap...]
where the time goes in v5:
time: 73.7 us; the launch traced here: 73.6 us
  Pallas kernels  72.9 us (99%)
    pallas_call x1, Pallas kernels, layer(): pl.pallas_call(functools.partial(layer_kernel, experts, splits), out_shap...  71.1 us
    pallas_call x1, Pallas kernels, export(): pl.pallas_call(export_kernel, out_shape=tuple((jax.ShapeDtypeStruct(a.sha...  1.83 us

profile of v5, /device:TPU:0, one launch (start us, length us, event | category | flops | bytes accessed | tf_op | source)
XLA Modules:
  0.0 73.6 jit_solution(14074504380401041342)
XLA Ops:
  0.6 71.1 %shard_map.134 = (bf16[128,1024]{1,0:T(8,128)(2,1)S(1)}, bf16[2,128]{1,0:T(2,128)(2,1)S(1)}, bf16[2048,256]{1,0:T(8,128)(2,1)S(1)}, bf16[2048,256]{1,0:T(8,128)(...) custom-call(s32[2,128]{1,0:T(2,128)} %bitcast.12, ...), custom_call_target="tpu_custom_call" | custom-call | tf_op jit(solution)/shard_map/pallas_call | solution.py:622
  71.7 1.8 %shard_map.135 = (bf16[128,1024]{1,0:T(8,128)(2,1)}, bf16[2,128]{1,0:T(2,128)(2,1)}, bf16[2048,256]{1,0:T(8,128)(2,1)}, bf16[2048,256]{1,0:T(8,128)(2,1)}, f32[1...) custom-call(bf16[128,1024]{1,0:T(8,128)(2,1)S(1)} %get-tuple-element.24.refs_0_, ...), custom_call_target="tpu_custom_call" | custom-call | tf_op jit(solution)/shard_map/pallas_call | solution.py:697

commit v6 on v5

--- a/solution.py
+++ b/solution.py
@@ -13,7 +13,7 @@
 TILE = 256
 GROUPS = 4
 HALVES = 2
-WHOLE = ((0, 1, 0, 0), (1, 1, 1, 1), (0, 0, 0, 0), (1, 1, 1, 1))
+WHOLE = ((0, 0, 0, 0), (1, 1, 1, 1), (0, 0, 0, 0), (1, 1, 1, 1))
 PLAN = (
     "far11", "far23", "spread03", "far22", "far21", "spread01", "spread00", "spread02", "fwd03",
     "far12", "spread23", "far20", "spread22", "far10", "fwd01", "far13", "far32", "fwd02", "spread11",

time: 73.7 us -> 73.7 us (level)
  no operation moved by 1% of the time
where the time goes in v6:
time: 73.7 us; the launch traced here: 73.6 us
  Pallas kernels  72.9 us (99%)
    pallas_call x1, Pallas kernels, layer(): pl.pallas_call(functools.partial(layer_kernel, experts, splits), out_shap...  71.1 us
    pallas_call x1, Pallas kernels, export(): pl.pallas_call(export_kernel, out_shape=tuple((jax.ShapeDtypeStruct(a.sha...  1.83 us

profile of v6, /device:TPU:0, one launch (start us, length us, event | category | flops | bytes accessed | tf_op | source)
XLA Modules:
  0.0 73.6 jit_solution(15200370224766668625)
XLA Ops:
  0.6 71.1 %shard_map.134 = (bf16[128,1024]{1,0:T(8,128)(2,1)S(1)}, bf16[2,128]{1,0:T(2,128)(2,1)S(1)}, bf16[2048,256]{1,0:T(8,128)(2,1)S(1)}, bf16[2048,256]{1,0:T(8,128)(...) custom-call(s32[2,128]{1,0:T(2,128)} %bitcast.12, ...), custom_call_target="tpu_custom_call" | custom-call | tf_op jit(solution)/shard_map/pallas_call | solution.py:622
  71.7 1.8 %shard_map.135 = (bf16[128,1024]{1,0:T(8,128)(2,1)}, bf16[2,128]{1,0:T(2,128)(2,1)}, bf16[2048,256]{1,0:T(8,128)(2,1)}, bf16[2048,256]{1,0:T(8,128)(2,1)}, f32[1...) custom-call(bf16[128,1024]{1,0:T(8,128)(2,1)S(1)} %get-tuple-element.24.refs_0_, ...), custom_call_target="tpu_custom_call" | custom-call | tf_op jit(solution)/shard_map/pallas_call | solution.py:697
